TPU v7x, 256 devices: a whole 4x4x8 slice. The times are simulated.
256 devices in a mesh: sp: 64 (over z, y, core), tp: 4 (over x).
Axes of the slice: x: 4, y: 4, z: 8, core: 2. Of those that a mesh axis runs over, the one named last changes fastest.
Arguments:
- tokens: bfloat16 [65536, 2048], P('sp'), may hold values from -6 to 6
- norm_gain: float32 [2048], replicated, may hold values from 0.1 to 1.9
- w_query: bfloat16 [2048, 1024], P('sp', 'tp'), may hold values from -3.5 to 3.5
- w_key: bfloat16 [2048, 256], P('sp', 'tp'), may hold values from -0.125 to 0.125
- w_value: bfloat16 [2048, 256], P('sp', 'tp'), may hold values from -0.125 to 0.125
- w_content: bfloat16 [2048, 1024], P('sp', 'tp'), may hold values from -0.125 to 0.125
- w_gate: bfloat16 [2048, 1024], P('sp', 'tp'), may hold values from -0.125 to 0.125
- sink_logit: float32 [16], P('tp'), may hold values from 1 to 6
- conv_weight: float32 [31, 1024], P(None, 'tp'), may hold values from -10 to 10
- conv_bias: float32 [1024], P('tp'), may hold values from 0 to 20
- channel_gain: float32 [1024], P('tp'), may hold values from 0.1 to 1.9
- out_attn: bfloat16 [1024, 2048], P('tp', 'sp'), may hold values from -0.75 to 0.75
- out_conv: bfloat16 [1024, 2048], P('tp', 'sp'), may hold values from -0.1875 to 0.1875
Outputs:
- mixed: bfloat16 [65536, 2048], P(('sp', 'tp'))
All inputs are finite; a program needn't handle non-finite values.
Results may differ from a plain program's by a relative error of at most 0.025.
The roundings to bfloat16 on the way count: a program that leaves them out, or rounds other values in their place, can miss the bound.
Values may be sent and summed in bfloat16 or wider, within the bound.
No kernel may reach another device: no remote copies, remote signals or barrier semaphores. Data moves between devices by JAX's collectives and lax.ppermute only.
A program may use at most 64 MiB of HBM per device.

v0:
```python
import functools

import jax
import jax.numpy as jnp
import numpy as np
from jax import lax
from jax.experimental import pallas as pl
from jax.experimental.pallas import tpu as pltpu
from jax.sharding import Mesh
from jax.sharding import PartitionSpec as P


HEAD_DIM = 64
CONV_CH = 1024
KERNEL = 31
WINDOW = 128
EPS = 1e-05
THETA = 10000.0
SP = ("z", "y", "c")
NX = 4
F32 = jnp.float32
BF16 = jnp.bfloat16


OWN = [(0, 0, 0, 0, 0)]


def to_partner(v, table):
    out = lax.ppermute(v, "c", [(0, 1), (1, 0)])
    return out, [(-a, -b, d ^ 1, e, -f) for a, b, d, e, f in table]


def onward(v, table, axis):
    size = lax.axis_size(axis)
    route = []
    for i in range(size):
        up, down = (i + 1) % size, (i - 1) % size
        if axis == "x":
            route += [(i, up), (size + i, size + down)]
        else:
            route += [(i * 2, up * 2), (i * 2 + 1, down * 2 + 1)]
    out = lax.ppermute(v, ("c", "x") if axis == "x" else (axis, "c"), route)
    k = {"z": 0, "y": 1, "x": 4}[axis]
    return out, [t[:k] + (t[k] - 1,) + t[k + 1 :] for t in table]


def go_round(v, table, axis):
    got = []
    for _ in range(lax.axis_size(axis) // 2):
        v, table = onward(v, table, axis)
        got.append((v, table))
    return got


def copy_kernel(plan, n_in, *refs):
    sources, results = refs[:n_in], refs[n_in:]
    for out, row, lane, src, row_0, lane_0, rows, lanes in plan:
        results[out][row : row + rows, lane : lane + lanes] = sources[src][row_0 : row_0 + rows, lane_0 : lane_0 + lanes]


def copied(sources, plan, shapes):
    outs = kernel_call(
        functools.partial(copy_kernel, plan, len(sources)),
        out_shape=tuple(jax.ShapeDtypeStruct(shape, BF16) for shape in shapes),
        in_specs=vmem(len(sources)),
        out_specs=tuple(vmem(len(shapes))),
        compiler_params=params(4),
        cost_estimate=cost(1 << 20, 1 << 20),
    )(*sources)
    return list(outs)


def join(parts, lo=0, hi=None):
    hi = hi or parts[0][0].shape[1]
    plan, row = [], 0
    for k, (v, _) in enumerate(parts):
        plan.append((0, row, 0, k, 0, lo, v.shape[0], hi - lo))
        row += v.shape[0]
    out = copied([v for v, _ in parts], plan, [(row, hi - lo)])[0]
    return out, sum((t for _, t in parts), [])


def tables(parts):
    return tuple(tuple(t) for _, t in parts)


def shift(v, axis, r):
    size = lax.axis_size(axis)
    return lax.ppermute(v, axis, [(i, (i + r) % size) for i in range(size)])


def around_x(blocks):
    return [blocks[0]] + [shift(blocks[r], "x", r) for r in range(1, NX)]


def around_y(v, table):
    return [(v, table)] + [(shift(v, "y", r), [(a, b, d, e - r, f) for a, b, d, e, f in table]) for r in (1, 3, 2)]


def kernel_call(body, **keys):
    return pl.pallas_call(body, **keys)


def vmem(n):
    return [pl.BlockSpec(memory_space=pltpu.VMEM)] * n


SMEM = pl.BlockSpec(memory_space=pltpu.SMEM)


def params(mib):
    return pltpu.CompilerParams(vmem_limit_bytes=mib * 1024 * 1024)


def put_rows(table, piece_refs, w_ref, across=False):
    z, y, c = (lax.axis_index(a) for a in SP)
    s = 1 - 2 * c
    for ref, places in zip(piece_refs, table):
        width = min(w_ref.shape[1], ref.shape[1])
        lane = pl.multiple_of(((-s * places[0][4]) & 3) * width, 128) if across else 0
        for k, (a, b, d, e, _) in enumerate(places):
            block = ((z + s * a) & 7) * 8 + ((y + s * b + e) & 3) * 2 + (c ^ d)
            row = pl.multiple_of(block * 32, 32)
            w_ref[pl.ds(row, 32), pl.ds(lane, width)] = ref[32 * k : 32 * k + 32, 0:width]


def lane_is(shape, period, limit):
    return lax.broadcasted_iota(jnp.int32, shape, len(shape) - 1) % period < limit


def sp_place():
    return (lax.axis_index("z") * 4 + lax.axis_index("y")) * 2 + lax.axis_index("c")


def turn(x, cosine, sine):
    other = jnp.where(lane_is(x.shape, 64, 32), pltpu.roll(x, 96, 1), pltpu.roll(x, 32, 1))
    return x * cosine + other * sine


def prep_kernel(tokens_ref, prior_ref, gain_ref, scaled_ref, inv_ref):
    def scale(wide, i):
        rows = pl.ds(pl.multiple_of(i * 32, 32), 32)
        scaled_ref[rows, :] = (wide * gain_ref[...]).astype(BF16)
        mean = jnp.sum(wide * wide, axis=1, keepdims=True) * (1.0 / wide.shape[1])
        inv_ref[rows, :] = jnp.broadcast_to(lax.rsqrt(mean + EPS), (32, 128))

    def before(i, _):
        scale(prior_ref[pl.ds(pl.multiple_of(i * 32, 32), 32), :].astype(F32), i)
        return 0

    def tile(i, _):
        scale(tokens_ref[pl.ds(pl.multiple_of(i * 32, 32), 32), :].astype(F32), i + WINDOW // 32)
        return 0

    lax.fori_loop(0, WINDOW // 32, before, 0)
    lax.fori_loop(0, tokens_ref.shape[0] // 32, tile, 0, unroll=2)


def rope_tables():
    half = HEAD_DIM // 2
    inverse = np.tile(1.0 / THETA ** (np.arange(half) * 2.0 / HEAD_DIM), 4)[None, :]
    steps = np.concatenate([np.arange(32), 1024 * np.arange(64), 32 * np.arange(-4, 36)])[:, None]
    return jnp.asarray(np.cos(steps * inverse), F32), jnp.asarray(np.sin(steps * inverse), F32)


def times_inv(out, inv):
    return jnp.concatenate([out[:, k : k + 128] * inv for k in range(0, out.shape[1], 128)], 1)


def qkv_kernel(table, *refs):
    n_pieces = len(table)
    pieces = refs[:n_pieces]
    x_ref, inv_ref, cos_ref, sin_ref, q_ref, kv_ref, w_ref = refs[n_pieces:]
    put_rows(table, pieces, w_ref)
    sp = sp_place()
    size = 384

    def tile(i, _):
        rows = pl.ds(pl.multiple_of(i * size, 128), size)
        out = jnp.dot(x_ref[rows, :], w_ref[...], preferred_element_type=F32)
        out = times_inv(out, inv_ref[rows, :])
        ca, sa = cos_ref[pl.ds(32 + sp, 1), :], sin_ref[pl.ds(32 + sp, 1), :]
        cl, sl = cos_ref[0:32, :], sin_ref[0:32, :]
        cosines, sines = [], []
        for j in range(size // 32):
            at = pl.ds(96 + i * (size // 32) + j, 1)
            cb, sb = cos_ref[at, :], sin_ref[at, :]
            ch, sh = ca * cb - sa * sb, sa * cb + ca * sb
            cosines.append(ch * cl - sh * sl)
            sines.append(sh * cl + ch * sl)
        cosine, sine = jnp.concatenate(cosines, 0), jnp.concatenate(sines, 0)
        sine = jnp.where(lane_is(sine.shape, 64, 32), -sine, sine)
        for p in range(2):
            turned = turn(out[:, p * 128 : p * 128 + 128], cosine, sine).astype(BF16)
            q_ref[rows, p * 128 : p * 128 + 128] = turned * BF16(HEAD_DIM**-0.5)
        kv = out[:, 256:384]
        vk = pltpu.roll(kv, 64, 1)
        first = lane_is(kv.shape, 128, 64)
        kv_ref[rows, 0:128] = turn(jnp.where(first, kv, vk), cosine, sine).astype(BF16)
        kv_ref[rows, 128:256] = jnp.where(first, vk, kv).astype(BF16)
        return 0

    lax.fori_loop(0, x_ref.shape[0] // size, tile, 0)


def glu_kernel(table, *refs):
    n_pieces = len(table)
    pieces = refs[:n_pieces]
    x_ref, inv_ref, glu_ref, w_ref = refs[n_pieces:]
    put_rows(table, pieces, w_ref)
    size = 384

    def tile(i, _):
        rows = pl.ds(pl.multiple_of(i * size, 128), size)
        out = jnp.dot(x_ref[rows, :], w_ref[...], preferred_element_type=F32)
        out = times_inv(out, inv_ref[rows, :])
        glu_ref[rows, :] = (out[:, :256] * jax.nn.sigmoid(out[:, 256:])).astype(BF16)
        return 0

    lax.fori_loop(0, x_ref.shape[0] // size, tile, 0)


def attention_kernel(sink_ref, q_ref, kv_ref, *refs):
    block_refs, (k_ref, v_ref, out_ref) = refs[:NX], refs[NX:]
    tokens = q_ref.shape[0] - WINDOW
    for half in range(2):
        for src, dst in ((kv_ref, 0),):
            rows = src.shape[0]
            keep = lane_is((rows, 128), 128, 64)
            if half:
                keep = jnp.logical_not(keep)
            zero = jnp.zeros((rows, 128), BF16)
            k_ref[half, dst : dst + rows, :] = jnp.where(keep, src[:, 0:128], zero)
            v_ref[half, dst : dst + rows, :] = jnp.where(keep, src[:, 128:256], zero)
    row = lax.broadcasted_iota(jnp.int32, (128, 256), 0)
    col = lax.broadcasted_iota(jnp.int32, (128, 256), 1)
    band = (col > row) & (col <= row + 128)

    def block(b, _):
        at = pl.multiple_of(b * 128, 128)
        lowest = jnp.where((b == 0) & (sp_place() == 0), WINDOW, 0)
        allowed = band & (col >= lowest)
        for pair in range(2):
            q = q_ref[pl.ds(at + WINDOW, 128), pair * 128 : pair * 128 + 128]
            total = None
            for half in range(2):
                scores = lax.dot_general(
                    q, k_ref[half, pl.ds(at, 256), :], (((1,), (1,)), ((), ())), preferred_element_type=F32
                )
                scores = jnp.where(allowed, scores, -1e30)
                sink = sink_ref[pair * 2 + half]
                row_max = jnp.maximum(jnp.max(scores, axis=1, keepdims=True), sink)
                weights = jnp.exp(scores - row_max)
                denominator = jnp.sum(weights, axis=1, keepdims=True) + jnp.exp(sink - row_max)
                probability = (weights * (1.0 / denominator)).astype(BF16)
                part = jnp.dot(probability, v_ref[half, pl.ds(at, 256), :], preferred_element_type=F32)
                total = part if total is None else total + part
            out_ref[pl.ds(at, 128), pair * 128 : pair * 128 + 128] = total.astype(BF16)
        return 0

    lax.fori_loop(0, tokens // 128, block, 0, unroll=2)
    to_blocks(out_ref, block_refs)


def to_blocks(src_ref, block_refs):
    share = src_ref.shape[0] // NX
    for r, ref in enumerate(block_refs):
        at = pl.multiple_of(((lax.axis_index("x") + r) & 3) * share, share)
        ref[0:share, :] = src_ref[pl.ds(at, share), :]


def conv_kernel(glu_ref, w_ref, bias_ref, gain_ref, *refs):
    block_refs, (shift_ref, out_ref) = refs[:NX], refs[NX:]
    tokens = glu_ref.shape[0] - WINDOW
    shift_ref[0, 0 : 32 + tokens, :] = glu_ref[WINDOW - 32 :, :].astype(F32)

    def fill(i, _):
        at = pl.multiple_of(i * 32, 32)
        rows = shift_ref[0, pl.ds(at, 40), :]
        for b in range(1, 8):
            shift_ref[b, pl.ds(at, 32), :] = rows[b : b + 32, :]
        return 0

    lax.fori_loop(0, tokens // 32 + 1, fill, 0)

    def tile(i, _):
        at = pl.multiple_of(i * 32, 32)
        total = None
        for j in range(KERNEL):
            ahead, b = divmod(j + 2, 8)
            term = w_ref[j : j + 1, :] * shift_ref[b, pl.ds(at + ahead * 8, 32), :]
            total = term if total is None else total + term
        out_ref[pl.ds(at, 32), :] = total.astype(BF16)
        return 0

    lax.fori_loop(0, tokens // 32, tile, 0)
    to_blocks(out_ref, block_refs)
    edge = jnp.concatenate([bias_ref[...], gain_ref[...]], 0)
    high = edge.astype(BF16).astype(F32)
    middle = (edge - high).astype(BF16).astype(F32)
    low = edge - high - middle
    rows = jnp.concatenate([high, middle, low, jnp.zeros((16 - 3 * edge.shape[0], edge.shape[1]), F32)], 0).astype(BF16)
    for ref in block_refs:
        ref[ref.shape[0] - 16 :, :] = rows


def out_attn_kernel(table, *refs):
    n_pieces = len(table)
    pieces, refs = refs[:n_pieces], refs[n_pieces:]
    attn, (out_ref, w_ref, act_ref) = refs[:NX], refs[NX:]
    put_rows(table, pieces, w_ref)
    wide = attn[0].shape[1]
    for r in range(NX):
        act_ref[:, r * wide : (r + 1) * wide] = attn[r][...]

    def tile(i, _):
        at = pl.multiple_of(i * 256, 256)
        out_ref[:, pl.ds(at, 256)] = lax.dot_general(
            act_ref[...], w_ref[pl.ds(at, 256), :], (((1,), (1,)), ((), ())), preferred_element_type=F32
        )
        return 0

    lax.fori_loop(0, out_ref.shape[1] // 256, tile, 0)


def out_conv_kernel(table, *refs):
    n_pieces = len(table)
    pieces, refs = refs[:n_pieces], refs[n_pieces:]
    conv, (partial_ref, out_ref, w_ref, act_ref) = refs[:NX], refs[NX:]
    put_rows(table, pieces, w_ref, across=True)
    rows, wide = conv[0].shape[0] - 16, conv[0].shape[1]
    sums, gains = [], []
    for r in range(NX):
        edge = conv[r][rows : rows + 16, :].astype(F32)
        sums.append(conv[r][0:rows, :].astype(F32) + (edge[0:1] + edge[2:3] + edge[4:5]))
        gains.append(edge[1:2] + edge[3:4] + edge[5:6])
    centre = sum(jnp.sum(s, axis=1, keepdims=True) for s in sums) * (1.0 / CONV_CH)
    centred = [s - centre for s in sums]
    variance = sum(jnp.sum(s * s, axis=1, keepdims=True) for s in centred) * (1.0 / CONV_CH)
    scale = lax.rsqrt(variance + EPS)
    for r in range(NX):
        value = centred[r] * scale * gains[r]
        act_ref[:, r * wide : (r + 1) * wide] = (value * jax.nn.sigmoid(value)).astype(BF16)

    def tile(i, _):
        at = pl.multiple_of(i * 256, 256)
        out = lax.dot_general(
            act_ref[...], w_ref[pl.ds(at, 256), :], (((1,), (1,)), ((), ())), preferred_element_type=F32
        )
        out_ref[:, pl.ds(at, 256)] = (out + partial_ref[:, pl.ds(at, 256)]).astype(BF16)
        return 0

    lax.fori_loop(0, out_ref.shape[1] // 256, tile, 0)


def cost(flops, moved):
    return pl.CostEstimate(flops=flops, bytes_accessed=moved, transcendentals=0)


def shards(
    tokens, norm_gain, w_query, w_key, w_value, w_content, w_gate, sink_logit,
    conv_weight, conv_bias, channel_gain, out_attn, out_conv,
):
    count = tokens.shape[0]
    n_qkv = w_query.shape[1] + w_key.shape[1] + w_value.shape[1]
    n_in = n_qkv + w_content.shape[1] + w_gate.shape[1]

    wide = out_attn.shape[0]
    own_in = jnp.concatenate([w_query, w_key, w_value, w_content, w_gate, out_conv.T], 1)
    lines = around_y(own_in, OWN)
    beside = around_x([out_attn.T] * NX)
    prior = lax.ppermute(tokens[count - WINDOW :], SP, [(i, i + 1) for i in range(63)])
    width_1, width_2 = n_qkv + wide, n_in - n_qkv + wide
    plan = []
    for k in range(4):
        plan.append((0, 32 * k, 0, k, 0, 0, 32, n_qkv))
        plan.append((0, 32 * k, n_qkv, 4 + k, 0, 0, 32, wide))
        plan.append((1, 32 * k, 0, k, 0, n_qkv, 32, width_2))
    mine = copied([v for v, _ in lines] + beside, plan, [(128, width_1), (128, width_2)])
    table = sum((t for _, t in lines), [])
    parts = []
    for k, part in enumerate(mine, 1):
        block = join([(part, table), to_partner(part, table)])
        got = go_round(*block, "z")
        far = join(got[:3])
        parts.append([block, far, got[3], to_partner(*far)])
    qkv_parts, cg_parts = parts

    plan, table = [], []
    marks = [(0, 1), (-1, 3), (-4, 1), (1, 3)]
    row = 0
    for piece, (first, count_z) in enumerate(marks):
        for n in range(count_z):
            at_z = first - n if first < 0 else first + n
            for h in range(2):
                for k in range(4):
                    plan.append((0, row, wide * k, piece, 256 * n + 128 * h + 32 * k, n_qkv, 32, wide))
                table.append((at_z, 0, h ^ (piece == 3), 0, 0))
                row += 32
    block = (copied([v for v, _ in qkv_parts], plan, [(row, 4 * wide)])[0], table)
    got = go_round(*block, "y")
    attn_parts = [block, got[0], got[1], to_partner(*got[0])]

    def cut(part, lo, hi):
        return part[0][lo:hi], part[1][lo // 32 : hi // 32]

    plan, table, row = [], [], 0
    for piece, lo, hi in ((0, 0, 128), (1, 0, 768), (2, 0, 128), (0, 128, 256), (2, 128, 256), (3, 0, 768)):
        plan.append((0, row, 0, piece, lo, n_in - n_qkv, hi - lo, wide))
        table += cg_parts[piece][1][lo // 32 : hi // 32]
        row += hi - lo
    full = (copied([v for v, _ in cg_parts], plan, [(row, wide)])[0], table)
    got_0 = onward(*full, "x")
    got_1 = onward(*cut(got_0, 0, row // 2), "x")
    conv_parts = [full, got_0, got_1, to_partner(*got_0), to_partner(*got_1)]

    scaled, inv_rms = kernel_call(
        prep_kernel,
        out_shape=(
            jax.ShapeDtypeStruct((WINDOW + count, tokens.shape[1]), BF16),
            jax.ShapeDtypeStruct((WINDOW + count, 128), F32),
        ),
        in_specs=vmem(3),
        out_specs=tuple(vmem(2)),
        compiler_params=params(4),
        cost_estimate=cost(1 << 30, 8 << 20),
    )(tokens, prior, norm_gain.reshape(1, -1))

    pieces = [v for v, _ in qkv_parts]
    queries, keys_values = kernel_call(
        functools.partial(qkv_kernel, tables(qkv_parts)),
        out_shape=(jax.ShapeDtypeStruct((WINDOW + count, 256), BF16),) * 2,
        in_specs=vmem(len(pieces) + 4),
        out_specs=tuple(vmem(2)),
        scratch_shapes=[pltpu.VMEM((2048, n_qkv), BF16)],
        compiler_params=params(8),
        cost_estimate=cost(2 * count * 2048 * 384, 8 << 20),
    )(*pieces, scaled, inv_rms, *rope_tables())
    glu = kernel_call(
        functools.partial(glu_kernel, tables(cg_parts)),
        out_shape=jax.ShapeDtypeStruct((WINDOW + count, 256), BF16),
        in_specs=vmem(len(cg_parts) + 2),
        out_specs=vmem(1)[0],
        scratch_shapes=[pltpu.VMEM((2048, n_in - n_qkv), BF16)],
        compiler_params=params(8),
        cost_estimate=cost(2 * count * 2048 * 512, 8 << 20),
    )(*[v for v, _ in cg_parts], scaled, inv_rms)

    share = count // NX
    attn_blocks = kernel_call(
        attention_kernel,
        out_shape=tuple([jax.ShapeDtypeStruct((share, 256), BF16)] * NX),
        in_specs=[SMEM] + vmem(2),
        out_specs=tuple(vmem(NX)),
        scratch_shapes=[pltpu.VMEM((2, WINDOW + count, 128), BF16)] * 2 + [pltpu.VMEM((count, 256), BF16)],
        compiler_params=params(8),
        cost_estimate=cost(2 * count * 2048 * 512, 8 << 20),
    )(sink_logit, queries, keys_values)
    attn_blocks = around_x(attn_blocks)

    conv_blocks = kernel_call(
        conv_kernel,
        out_shape=tuple([jax.ShapeDtypeStruct((share + 16, 256), BF16)] * NX),
        in_specs=vmem(4),
        out_specs=tuple(vmem(NX)),
        scratch_shapes=[pltpu.VMEM((8, count + 48, 256), F32), pltpu.VMEM((count, 256), BF16)],
        compiler_params=params(16),
        cost_estimate=cost(2 * count * 2048 * 512, 8 << 20),
    )(glu, conv_weight, conv_bias.reshape(1, -1), channel_gain.reshape(1, -1))
    conv_blocks = around_x(conv_blocks)

    partial_sum = kernel_call(
        functools.partial(out_attn_kernel, tables(attn_parts)),
        out_shape=jax.ShapeDtypeStruct((share, 2048), F32),
        in_specs=vmem(len(attn_parts) + NX),
        out_specs=vmem(1)[0],
        scratch_shapes=[pltpu.VMEM((2048, 1024), BF16), pltpu.VMEM((share, 1024), BF16)],
        compiler_params=params(8),
        cost_estimate=cost(256 * 2048 * 2048, 6 << 20),
    )(*[v for v, _ in attn_parts], *attn_blocks)
    return kernel_call(
        functools.partial(out_conv_kernel, tables(conv_parts)),
        out_shape=jax.ShapeDtypeStruct((share, 2048), BF16),
        in_specs=vmem(len(conv_parts) + NX + 1),
        out_specs=vmem(1)[0],
        scratch_shapes=[pltpu.VMEM((2048, 1024), BF16), pltpu.VMEM((share, 1024), BF16)],
        compiler_params=params(10),
        cost_estimate=cost(256 * 2048 * 2048, 6 << 20),
    )(*[v for v, _ in conv_parts], *conv_blocks, partial_sum)


def solution(mesh):
    torus = Mesh(mesh.devices.reshape(8, 4, 2, mesh.shape["tp"]), ("z", "y", "c", "x"))
    return jax.shard_map(
        shards,
        mesh=torus,
        in_specs=(
            P(SP, None), P(), P(SP, "x"), P(SP, "x"), P(SP, "x"), P(SP, "x"), P(SP, "x"), P("x"),
            P(None, "x"), P("x"), P("x"), P("x", SP), P("x", SP),
        ),
        out_specs=P((*SP, "x"), None),
        check_vma=False,
    )
```

profile of v0, /device:TPU:1, one launch (start us, length us, event | category | flops | bytes accessed | tf_op | source)
XLA Modules:
  0.0 133.9 jit_solution(5601394555194128567)
XLA Ops:
  0.9 2.2 %collective-permute-start = (bf16[32,1152]{1,0:T(8,128)(2,1)S(1)}, bf16[32,1152]{1,0:T(8,128)(2,1)S(1)}, u32[]{:S(2)}, u32[]{:S(2)}) collective-permute-start(bf16[32,1152]{1,0:T(8,128)(2,1)S(1)} %concatenate.3.refs_0_), channel_id=1, source_target_pairs={{0,8},{8,16},{16,24},{24,0},{1,9},{9,17},{17,25},{25,1},{2,10},{10... | collective-permute-start | bytes 221192 | tf_op jit(solution)/shard_map/ppermute | solution.py:89
  3.1 1.5 %collective-permute-start.1 = (bf16[32,1152]{1,0:T(8,128)(2,1)S(1)}, bf16[32,1152]{1,0:T(8,128)(2,1)S(1)}, u32[]{:S(2)}, u32[]{:S(2)}) collective-permute-start(bf16[32,1152]{1,0:T(8,128)(2,1)S(1)} %concatenate.3.refs_0_), channel_id=1, source_target_pairs={{0,24},{8,0},{16,8},{24,16},{1,25},{9,1},{17,9},{25,17},{2,26},{10... | collective-permute-start | bytes 221192 | tf_op jit(solution)/shard_map/ppermute | solution.py:89
  4.6 1.6 %collective-permute-start.2 = (bf16[32,1152]{1,0:T(8,128)(2,1)S(1)}, bf16[32,1152]{1,0:T(8,128)(2,1)S(1)}, u32[]{:S(2)}, u32[]{:S(2)}) collective-permute-start(bf16[32,1152]{1,0:T(8,128)(2,1)S(1)} %concatenate.3.refs_0_), channel_id=1, source_target_pairs={{0,16},{8,24},{16,0},{24,8},{1,17},{9,25},{17,1},{25,9},{2,18},{10... | collective-permute-start | bytes 221192 | tf_op jit(solution)/shard_map/ppermute | solution.py:89
  7.4 2.5 %collective-permute-start.4 = (bf16[32,256]{1,0:T(8,128)(2,1)}, bf16[32,256]{1,0:T(8,128)(2,1)S(1)}, u32[]{:S(2)}, u32[]{:S(2)}) collective-permute-start(bf16[32,256]{1,0:T(8,128)(2,1)} %bitcast.6), channel_id=1, source_target_pairs={{0,2},{1,3},{2,0},{3,1},{4,6},{5,7},{6,4},{7,5},{8,10},{9,11},{10,... | collective-permute-start | bytes 49160 | tf_op jit(solution)/shard_map/ppermute | solution.py:89
  11.7 1.7 %collective-permute-done.5.refs_7_ = bf16[32,256]{1,0:T(8,128)(2,1)S(1)} collective-permute-done((bf16[32,256]{1,0:T(8,128)(2,1)}, bf16[32,256]{1,0:T(8,128)(2,1)S(1)}, u32[]{:S(2)}, u32[]{:S(2)}) %collective-permute-start.5) | collective-permute-done | bytes 16416 | tf_op jit(solution)/shard_map/ppermute | solution.py:89
  14.2 3.5 %collective-permute-start.6 = (bf16[128,768]{1,0:T(8,128)(2,1)S(1)}, bf16[128,768]{1,0:T(8,128)(2,1)S(1)}, u32[]{:S(2)}, u32[]{:S(2)}) collective-permute-start(bf16[128,768]{1,0:T(8,128)(2,1)S(1)} %get-tuple-element.19.refs_0_), channel_id=1, source_target_pairs={{0,4},{4,0},{1,5},{5,1},{2,6},{6,2},{3,7},{7,3},{8,12},{12,8},{9,1... | collective-permute-start | bytes 589832 | tf_op jit(solution)/shard_map/ppermute | solution.py:29
  18.7 5.7 %collective-permute-start.7 = (bf16[256,768]{1,0:T(8,128)(2,1)S(1)}, bf16[256,768]{1,0:T(8,128)(2,1)S(1)}, u32[]{:S(2)}, u32[]{:S(2)}) collective-permute-start(bf16[256,768]{1,0:T(8,128)(2,1)S(1)} %shard_map.146.refs_0_), channel_id=1, source_target_pairs={{0,32},{4,228},{32,64},{36,4},{64,96},{68,36},{96,128},{100,68},{1... | collective-permute-start | bytes 1179656 | tf_op jit(solution)/shard_map/ppermute | solution.py:42
  24.4 1.4 %collective-permute-done.20.refs_1_ = bf16[128,640]{1,0:T(8,128)(2,1)S(1)} collective-permute-done((bf16[128,640]{1,0:T(8,128)(2,1)S(1)}, bf16[128,640]{1,0:T(8,128)(2,1)S(1)}, u32[]{:S(2)}, u32[]{:S(2)}) %collective-permute-start.20) | collective-permute-done | bytes 163872 | tf_op jit(solution)/shard_map/ppermute | solution.py:29
  26.6 2.5 %collective-permute-done.7.refs_0_ = bf16[256,768]{1,0:T(8,128)(2,1)S(1)} collective-permute-done((bf16[256,768]{1,0:T(8,128)(2,1)S(1)}, bf16[256,768]{1,0:T(8,128)(2,1)S(1)}, u32[]{:S(2)}, u32[]{:S(2)}) %collective-permute-start.7) | collective-permute-done | bytes 393248 | tf_op jit(solution)/shard_map/ppermute | solution.py:42
  29.1 3.1 %collective-permute-start.8 = (bf16[256,768]{1,0:T(8,128)(2,1)S(1)}, bf16[256,768]{1,0:T(8,128)(2,1)S(1)}, u32[]{:S(2)}, u32[]{:S(2)}) collective-permute-start(bf16[256,768]{1,0:T(8,128)(2,1)S(1)} %collective-permute-done.7.refs_0_), channel_id=1, source_target_pairs={{0,32},{4,228},{32,64},{36,4},{64,96},{68,36},{96,128},{100,68},{1... | collective-permute-start | bytes 1179656 | tf_op jit(solution)/shard_map/ppermute | solution.py:42
  32.6 3.1 %collective-permute-start.22 = (bf16[256,640]{1,0:T(8,128)(2,1)S(1)}, bf16[256,640]{1,0:T(8,128)(2,1)S(1)}, u32[]{:S(2)}, u32[]{:S(2)}) collective-permute-start(bf16[256,640]{1,0:T(8,128)(2,1)S(1)} %collective-permute-done.21.refs_0_), channel_id=1, source_target_pairs={{0,32},{4,228},{32,64},{36,4},{64,96},{68,36},{96,128},{100,68},{1... | collective-permute-start | bytes 983048 | tf_op jit(solution)/shard_map/ppermute | solution.py:42
  37.0 3.1 %collective-permute-start.9 = (bf16[256,768]{1,0:T(8,128)(2,1)S(1)}, bf16[256,768]{1,0:T(8,128)(2,1)S(1)}, u32[]{:S(2)}, u32[]{:S(2)}) collective-permute-start(bf16[256,768]{1,0:T(8,128)(2,1)S(1)} %collective-permute-done.8.refs_1_), channel_id=1, source_target_pairs={{0,32},{4,228},{32,64},{36,4},{64,96},{68,36},{96,128},{100,68},{1... | collective-permute-start | bytes 1179656 | tf_op jit(solution)/shard_map/ppermute | solution.py:42
  40.5 3.1 %collective-permute-start.23 = (bf16[256,640]{1,0:T(8,128)(2,1)S(1)}, bf16[256,640]{1,0:T(8,128)(2,1)S(1)}, u32[]{:S(2)}, u32[]{:S(2)}) collective-permute-start(bf16[256,640]{1,0:T(8,128)(2,1)S(1)} %collective-permute-done.22.refs_1_), channel_id=1, source_target_pairs={{0,32},{4,228},{32,64},{36,4},{64,96},{68,36},{96,128},{100,68},{1... | collective-permute-start | bytes 983048 | tf_op jit(solution)/shard_map/ppermute | solution.py:42
  44.9 4.1 %collective-permute-start.11 = (bf16[768,768]{1,0:T(8,128)(2,1)S(1)}, bf16[768,768]{1,0:T(8,128)(2,1)S(1)}, u32[]{:S(2)}, u32[]{:S(2)}) collective-permute-start(bf16[768,768]{1,0:T(8,128)(2,1)S(1)} %shard_map.147.refs_1_), channel_id=1, source_target_pairs={{0,4},{4,0},{1,5},{5,1},{2,6},{6,2},{3,7},{7,3},{8,12},{12,8},{9,1... | collective-permute-start | bytes 3538952 | tf_op jit(solution)/shard_map/ppermute | solution.py:29
  49.0 3.4 %collective-permute-start.25 = (bf16[768,640]{1,0:T(8,128)(2,1)S(1)}, bf16[768,640]{1,0:T(8,128)(2,1)S(1)}, u32[]{:S(2)}, u32[]{:S(2)}) collective-permute-start(bf16[768,640]{1,0:T(8,128)(2,1)S(1)} %shard_map.153.refs_1_), channel_id=1, source_target_pairs={{0,4},{4,0},{1,5},{5,1},{2,6},{6,2},{3,7},{7,3},{8,12},{12,8},{9,1... | collective-permute-start | bytes 2949128 | tf_op jit(solution)/shard_map/ppermute | solution.py:29
  52.5 10.4 %collective-permute-done.24.refs_2_ = bf16[256,640]{1,0:T(8,128)(2,1)S(1)} collective-permute-done((bf16[256,640]{1,0:T(8,128)(2,1)S(1)}, bf16[256,640]{1,0:T(8,128)(2,1)S(1)}, u32[]{:S(2)}, u32[]{:S(2)}) %collective-permute-start.24) | collective-permute-done | bytes 327712 | tf_op jit(solution)/shard_map/ppermute | solution.py:42
  63.9 2.6 %collective-permute-start.12 = (bf16[2048,256]{1,0:T(8,128)(2,1)S(1)}, bf16[2048,256]{1,0:T(8,128)(2,1)S(1)}, u32[]{:S(2)}, u32[]{:S(2)}) collective-permute-start(bf16[2048,256]{1,0:T(8,128)(2,1)S(1)} %shard_map.148.refs_0_), channel_id=1, source_target_pairs={{0,1},{4,7},{1,2},{5,4},{2,3},{6,5},{3,0},{7,6},{8,9},{12,15},{9,1... | collective-permute-start | bytes 3145736 | tf_op jit(solution)/shard_map/ppermute | solution.py:42
  66.5 3.0 %collective-permute-start.16 = (bf16[128,2048]{1,0:T(8,128)(2,1)S(1)}, bf16[128,2048]{1,0:T(8,128)(2,1)S(1)}, u32[]{:S(2)}, u32[]{:S(2)}) collective-permute-start(bf16[128,2048]{1,0:T(8,128)(2,1)S(1)} %slice.7), channel_id=1, source_target_pairs={{0,4},{4,8},{8,12},{12,16},{16,20},{20,24},{24,28},{28,32},{32,36}... | collective-permute-start | bytes 1572872 | tf_op jit(solution)/shard_map/ppermute | solution.py:372
  69.5 7.4 %collective-permute-done.26.refs_1_ = bf16[512,1024]{1,0:T(8,128)(2,1)S(1)} collective-permute-done((bf16[512,1024]{1,0:T(8,128)(2,1)S(1)}, bf16[512,1024]{1,0:T(8,128)(2,1)S(1)}, u32[]{:S(2)}, u32[]{:S(2)}) %collective-permute-start.26) | collective-permute-done | bytes 1048608 | tf_op jit(solution)/shard_map/ppermute | solution.py:42
  77.0 2.0 %collective-permute-start.27 = (bf16[512,1024]{1,0:T(8,128)(2,1)S(1)}, bf16[512,1024]{1,0:T(8,128)(2,1)S(1)}, u32[]{:S(2)}, u32[]{:S(2)}) collective-permute-start(bf16[512,1024]{1,0:T(8,128)(2,1)S(1)} %collective-permute-done.26.refs_1_), channel_id=1, source_target_pairs={{0,8},{4,28},{8,16},{12,4},{16,24},{20,12},{24,0},{28,20},{1,9},{5... | collective-permute-start | bytes 3145736 | tf_op jit(solution)/shard_map/ppermute | solution.py:42
  79.0 7.3 %collective-permute-start.28 = (bf16[512,1024]{1,0:T(8,128)(2,1)S(1)}, bf16[512,1024]{1,0:T(8,128)(2,1)S(1)}, u32[]{:S(2)}, u32[]{:S(2)}) collective-permute-start(bf16[512,1024]{1,0:T(8,128)(2,1)S(1)} %collective-permute-done.26.refs_1_), channel_id=1, source_target_pairs={{0,4},{4,0},{1,5},{5,1},{2,6},{6,2},{3,7},{7,3},{8,12},{12,8},{9,1... | collective-permute-start | bytes 3145736 | tf_op jit(solution)/shard_map/ppermute | solution.py:29
  86.3 2.6 %collective-permute-start.13 = (bf16[1024,256]{1,0:T(8,128)(2,1)S(1)}, bf16[1024,256]{1,0:T(8,128)(2,1)S(1)}, u32[]{:S(2)}, u32[]{:S(2)}) collective-permute-start(bf16[1024,256]{1,0:T(8,128)(2,1)S(1)} %slice.8), channel_id=1, source_target_pairs={{0,1},{4,7},{1,2},{5,4},{2,3},{6,5},{3,0},{7,6},{8,9},{12,15},{9,1... | collective-permute-start | bytes 1572872 | tf_op jit(solution)/shard_map/ppermute | solution.py:42
  88.9 3.3 %shard_map.149 = (bf16[1152,2048]{1,0:T(8,128)(2,1)S(1)}, f32[1152,128]{1,0:T(8,128)S(1)}) custom-call(bf16[1024,2048]{1,0:T(8,128)(2,1)S(1)} %copy-done, bf16[128,2048]{1,0:T(8,128)(2,1)S(1)} %collective-permute-done.16.prior_ref, f32[1,2048]{1,0:T(1,128)S(1)} %bitcast.9), custom_call_target="tpu_custom_call" | custom-call | flops 1073741824 | bytes 8388608 | tf_op jit(solution)/shard_map/pallas_call | solution.py:417
  92.3 4.2 %shard_map.155 = (bf16[1152,256]{1,0:T(8,128)(2,1)S(1)}, bf16[1152,256]{1,0:T(8,128)(2,1)S(1)}) custom-call(bf16[256,640]{1,0:T(8,128)(2,1)S(1)} %shard_map.152.refs_0_, bf16[768,640]{1,0:T(8,128)(2,1)S(1)} %shard_map.153.refs_1_, bf16[256,640]{1,0:T(8,128)(2,1)S(1)} %collective-permute-done.24.refs_2_, ...), custom_call_target="tpu_custom_call" | custom-call | flops 1610612736 | bytes 8388608 | tf_op jit(solution)/shard_map/pallas_call | solution.py:430
  96.5 7.0 %shard_map.156 = (bf16[256,256]{1,0:T(8,128)(2,1)S(1)}, bf16[256,256]{1,0:T(8,128)(2,1)S(1)}, bf16[256,256]{1,0:T(8,128)(2,1)S(1)}, bf16[256,256]{1,0:T(8,128)(2,1)S(1)}) custom-call(f32[4]{0:T(128)S(1)} %copy-done.8, bf16[1152,256]{1,0:T(8,128)(2,1)S(1)} %get-tuple-element.27.q_ref, bf16[1152,256]{1,0:T(8,128)(2,1)S(1)} %get-tuple-element.28.kv_ref), custom_call_target="tpu_custom_call" | custom-call | flops 2147483648 | bytes 8388608 | tf_op jit(solution)/shard_map/pallas_call | solution.py:450
  103.6 5.8 %collective-permute-done.29.refs_5_ = bf16[256,256]{1,0:T(8,128)(2,1)S(1)} collective-permute-done((bf16[256,256]{1,0:T(8,128)(2,1)S(1)}, bf16[256,256]{1,0:T(8,128)(2,1)S(1)}, u32[]{:S(2)}, u32[]{:S(2)}) %collective-permute-start.29) | collective-permute-done | bytes 131104 | tf_op jit(solution)/shard_map/ppermute | solution.py:89
  111.2 3.1 %shard_map.150.glu_ref = bf16[1152,256]{1,0:T(8,128)(2,1)S(1)} custom-call(bf16[256,768]{1,0:T(8,128)(2,1)S(1)} %shard_map.146.refs_0_, bf16[768,768]{1,0:T(8,128)(2,1)S(1)} %shard_map.147.refs_1_, bf16[256,768]{1,0:T(8,128)(2,1)S(1)} %collective-permute-done.10.refs_2_, bf16[768,768]{1,0:T(8,128)(2,1)S(1)} %collective-permute-done.11.refs_3_, ...), custom_call_target="tpu_custom_call" | custom-call | flops 2147483648 | bytes 8388608 | tf_op jit(solution)/shard_map/pallas_call | solution.py:439
  115.4 4.6 %shard_map.151 = (bf16[272,256]{1,0:T(8,128)(2,1)S(1)}, bf16[272,256]{1,0:T(8,128)(2,1)S(1)}, bf16[272,256]{1,0:T(8,128)(2,1)S(1)}, bf16[272,256]{1,0:T(8,128)(2,1)S(1)}) custom-call(bf16[1152,256]{1,0:T(8,128)(2,1)S(1)} %shard_map.150.glu_ref, f32[31,256]{1,0:T(8,128)S(1)} %copy-done.5, f32[1,256]{1,0:T(1,128)S(1)} %bitcast.10, f32[1,256]{1,0:T(1,128)S(1)} %bitcast.11), custom_call_target="tpu_custom_call" | custom-call | flops 2147483648 | bytes 8388608 | tf_op jit(solution)/shard_map/pallas_call | solution.py:461
  120.8 2.5 %collective-permute-start.18 = (bf16[272,256]{1,0:T(8,128)(2,1)S(1)}, bf16[272,256]{1,0:T(8,128)(2,1)S(1)}, u32[]{:S(2)}, u32[]{:S(2)}) collective-permute-start(bf16[272,256]{1,0:T(8,128)(2,1)S(1)} %get-tuple-element.24), channel_id=1, source_target_pairs={{0,2},{1,3},{2,0},{3,1},{4,6},{5,7},{6,4},{7,5},{8,10},{9,11},{10,... | collective-permute-start | bytes 417800 | tf_op jit(solution)/shard_map/ppermute | solution.py:89
  124.0 3.1 %shard_map.157.refs_9_ = f32[256,2048]{1,0:T(8,128)S(1)} custom-call(bf16[512,1024]{1,0:T(8,128)(2,1)S(1)} %shard_map.154.refs_0_, bf16[512,1024]{1,0:T(8,128)(2,1)S(1)} %collective-permute-done.26.refs_1_, bf16[512,1024]{1,0:T(8,128)(2,1)S(1)} %collective-permute-done.27.refs_2_, bf16[512,1024]{1,0:T(8,128)(2,1)S(1)} %collective-permute-done.28.refs_3_, ...), custom_call_target="tpu_custom_call" | custom-call | flops 1073741824 | bytes 6291456 | tf_op jit(solution)/shard_map/pallas_call | solution.py:472
  127.1 2.0 %collective-permute-done.18.refs_7_ = bf16[272,256]{1,0:T(8,128)(2,1)S(1)} collective-permute-done((bf16[272,256]{1,0:T(8,128)(2,1)S(1)}, bf16[272,256]{1,0:T(8,128)(2,1)S(1)}, u32[]{:S(2)}, u32[]{:S(2)}) %collective-permute-start.18) | collective-permute-done | bytes 139296 | tf_op jit(solution)/shard_map/ppermute | solution.py:89
  129.1 4.7 %shard_map.158 = bf16[256,2048]{1,0:T(8,128)(2,1)} custom-call(bf16[2048,256]{1,0:T(8,128)(2,1)S(1)} %shard_map.148.refs_0_, bf16[2048,256]{1,0:T(8,128)(2,1)S(1)} %collective-permute-done.12.refs_1_, bf16[1024,256]{1,0:T(8,128)(2,1)S(1)} %collective-permute-done.13.refs_2_, bf16[2048,256]{1,0:T(8,128)(2,1)S(1)} %collective-permute-done.14.refs_3_, ...), custom_call_target="tpu_custom_call" | custom-call | flops 1073741824 | bytes 6291456 | tf_op jit(solution)/shard_map/pallas_call | solution.py:481
  (67 shorter events, 15.7 us)
Async XLA Ops:
  0.9 12.5 %collective-permute-start = (bf16[32,1152]{1,0:T(8,128)(2,1)S(1)}, bf16[32,1152]{1,0:T(8,128)(2,1)S(1)}, u32[]{:S(2)}, u32[]{:S(2)}) collective-permute-start(bf16[32,1152]{1,0:T(8,128)(2,1)S(1)} %concatenate.3.refs_0_), channel_id=1, source_target_pairs={{0,8},{8,16},{16,24},{24,0},{1,9},{9,17},{17,25},{25,1},{2,10},{10... | collective-permute-start | bytes 221192 | tf_op jit(solution)/shard_map/ppermute | solution.py:89
  3.1 10.3 %collective-permute-start.1 = (bf16[32,1152]{1,0:T(8,128)(2,1)S(1)}, bf16[32,1152]{1,0:T(8,128)(2,1)S(1)}, u32[]{:S(2)}, u32[]{:S(2)}) collective-permute-start(bf16[32,1152]{1,0:T(8,128)(2,1)S(1)} %concatenate.3.refs_0_), channel_id=1, source_target_pairs={{0,24},{8,0},{16,8},{24,16},{1,25},{9,1},{17,9},{25,17},{2,26},{10... | collective-permute-start | bytes 221192 | tf_op jit(solution)/shard_map/ppermute | solution.py:89
  4.6 8.8 %collective-permute-start.2 = (bf16[32,1152]{1,0:T(8,128)(2,1)S(1)}, bf16[32,1152]{1,0:T(8,128)(2,1)S(1)}, u32[]{:S(2)}, u32[]{:S(2)}) collective-permute-start(bf16[32,1152]{1,0:T(8,128)(2,1)S(1)} %concatenate.3.refs_0_), channel_id=1, source_target_pairs={{0,16},{8,24},{16,0},{24,8},{1,17},{9,25},{17,1},{25,9},{2,18},{10... | collective-permute-start | bytes 221192 | tf_op jit(solution)/shard_map/ppermute | solution.py:89
  6.2 4.0 %collective-permute-start.3 = (bf16[32,256]{1,0:T(8,128)(2,1)}, bf16[32,256]{1,0:T(8,128)(2,1)S(1)}, u32[]{:S(2)}, u32[]{:S(2)}) collective-permute-start(bf16[32,256]{1,0:T(8,128)(2,1)} %bitcast.5), channel_id=1, source_target_pairs={{0,1},{1,2},{2,3},{3,0},{4,5},{5,6},{6,7},{7,4},{8,9},{9,10},{10,1... | collective-permute-start | bytes 49160 | tf_op jit(solution)/shard_map/ppermute | solution.py:89
  7.4 4.3 %collective-permute-start.4 = (bf16[32,256]{1,0:T(8,128)(2,1)}, bf16[32,256]{1,0:T(8,128)(2,1)S(1)}, u32[]{:S(2)}, u32[]{:S(2)}) collective-permute-start(bf16[32,256]{1,0:T(8,128)(2,1)} %bitcast.6), channel_id=1, source_target_pairs={{0,2},{1,3},{2,0},{3,1},{4,6},{5,7},{6,4},{7,5},{8,10},{9,11},{10,... | collective-permute-start | bytes 49160 | tf_op jit(solution)/shard_map/ppermute | solution.py:89
  10.2 3.2 %collective-permute-start.5 = (bf16[32,256]{1,0:T(8,128)(2,1)}, bf16[32,256]{1,0:T(8,128)(2,1)S(1)}, u32[]{:S(2)}, u32[]{:S(2)}) collective-permute-start(bf16[32,256]{1,0:T(8,128)(2,1)} %bitcast.7), channel_id=1, source_target_pairs={{0,3},{1,0},{2,1},{3,2},{4,7},{5,4},{6,5},{7,6},{8,11},{9,8},{10,9... | collective-permute-start | bytes 49160 | tf_op jit(solution)/shard_map/ppermute | solution.py:89
  14.2 4.5 %collective-permute-start.6 = (bf16[128,768]{1,0:T(8,128)(2,1)S(1)}, bf16[128,768]{1,0:T(8,128)(2,1)S(1)}, u32[]{:S(2)}, u32[]{:S(2)}) collective-permute-start(bf16[128,768]{1,0:T(8,128)(2,1)S(1)} %get-tuple-element.19.refs_0_), channel_id=1, source_target_pairs={{0,4},{4,0},{1,5},{5,1},{2,6},{6,2},{3,7},{7,3},{8,12},{12,8},{9,1... | collective-permute-start | bytes 589832 | tf_op jit(solution)/shard_map/ppermute | solution.py:29
  18.7 10.4 %collective-permute-start.7 = (bf16[256,768]{1,0:T(8,128)(2,1)S(1)}, bf16[256,768]{1,0:T(8,128)(2,1)S(1)}, u32[]{:S(2)}, u32[]{:S(2)}) collective-permute-start(bf16[256,768]{1,0:T(8,128)(2,1)S(1)} %shard_map.146.refs_0_), channel_id=1, source_target_pairs={{0,32},{4,228},{32,64},{36,4},{64,96},{68,36},{96,128},{100,68},{1... | collective-permute-start | bytes 1179656 | tf_op jit(solution)/shard_map/ppermute | solution.py:42
  24.4 1.4 %collective-permute-start.20 = (bf16[128,640]{1,0:T(8,128)(2,1)S(1)}, bf16[128,640]{1,0:T(8,128)(2,1)S(1)}, u32[]{:S(2)}, u32[]{:S(2)}) collective-permute-start(bf16[128,640]{1,0:T(8,128)(2,1)S(1)} %get-tuple-element.26.refs_0_), channel_id=1, source_target_pairs={{0,4},{4,0},{1,5},{5,1},{2,6},{6,2},{3,7},{7,3},{8,12},{12,8},{9,1... | collective-permute-start | bytes 491528 | tf_op jit(solution)/shard_map/ppermute | solution.py:29
  25.8 6.8 %collective-permute-start.21 = (bf16[256,640]{1,0:T(8,128)(2,1)S(1)}, bf16[256,640]{1,0:T(8,128)(2,1)S(1)}, u32[]{:S(2)}, u32[]{:S(2)}) collective-permute-start(bf16[256,640]{1,0:T(8,128)(2,1)S(1)} %shard_map.152.refs_0_), channel_id=1, source_target_pairs={{0,32},{4,228},{32,64},{36,4},{64,96},{68,36},{96,128},{100,68},{1... | collective-permute-start | bytes 983048 | tf_op jit(solution)/shard_map/ppermute | solution.py:42
  29.1 7.8 %collective-permute-start.8 = (bf16[256,768]{1,0:T(8,128)(2,1)S(1)}, bf16[256,768]{1,0:T(8,128)(2,1)S(1)}, u32[]{:S(2)}, u32[]{:S(2)}) collective-permute-start(bf16[256,768]{1,0:T(8,128)(2,1)S(1)} %collective-permute-done.7.refs_0_), channel_id=1, source_target_pairs={{0,32},{4,228},{32,64},{36,4},{64,96},{68,36},{96,128},{100,68},{1... | collective-permute-start | bytes 1179656 | tf_op jit(solution)/shard_map/ppermute | solution.py:42
  32.6 7.8 %collective-permute-start.22 = (bf16[256,640]{1,0:T(8,128)(2,1)S(1)}, bf16[256,640]{1,0:T(8,128)(2,1)S(1)}, u32[]{:S(2)}, u32[]{:S(2)}) collective-permute-start(bf16[256,640]{1,0:T(8,128)(2,1)S(1)} %collective-permute-done.21.refs_0_), channel_id=1, source_target_pairs={{0,32},{4,228},{32,64},{36,4},{64,96},{68,36},{96,128},{100,68},{1... | collective-permute-start | bytes 983048 | tf_op jit(solution)/shard_map/ppermute | solution.py:42
  37.0 7.8 %collective-permute-start.9 = (bf16[256,768]{1,0:T(8,128)(2,1)S(1)}, bf16[256,768]{1,0:T(8,128)(2,1)S(1)}, u32[]{:S(2)}, u32[]{:S(2)}) collective-permute-start(bf16[256,768]{1,0:T(8,128)(2,1)S(1)} %collective-permute-done.8.refs_1_), channel_id=1, source_target_pairs={{0,32},{4,228},{32,64},{36,4},{64,96},{68,36},{96,128},{100,68},{1... | collective-permute-start | bytes 1179656 | tf_op jit(solution)/shard_map/ppermute | solution.py:42
  40.5 8.5 %collective-permute-start.23 = (bf16[256,640]{1,0:T(8,128)(2,1)S(1)}, bf16[256,640]{1,0:T(8,128)(2,1)S(1)}, u32[]{:S(2)}, u32[]{:S(2)}) collective-permute-start(bf16[256,640]{1,0:T(8,128)(2,1)S(1)} %collective-permute-done.22.refs_1_), channel_id=1, source_target_pairs={{0,32},{4,228},{32,64},{36,4},{64,96},{68,36},{96,128},{100,68},{1... | collective-permute-start | bytes 983048 | tf_op jit(solution)/shard_map/ppermute | solution.py:42
  44.9 19.0 %collective-permute-start.11 = (bf16[768,768]{1,0:T(8,128)(2,1)S(1)}, bf16[768,768]{1,0:T(8,128)(2,1)S(1)}, u32[]{:S(2)}, u32[]{:S(2)}) collective-permute-start(bf16[768,768]{1,0:T(8,128)(2,1)S(1)} %shard_map.147.refs_1_), channel_id=1, source_target_pairs={{0,4},{4,0},{1,5},{5,1},{2,6},{6,2},{3,7},{7,3},{8,12},{12,8},{9,1... | collective-permute-start | bytes 3538952 | tf_op jit(solution)/shard_map/ppermute | solution.py:29
  49.0 13.9 %collective-permute-start.25 = (bf16[768,640]{1,0:T(8,128)(2,1)S(1)}, bf16[768,640]{1,0:T(8,128)(2,1)S(1)}, u32[]{:S(2)}, u32[]{:S(2)}) collective-permute-start(bf16[768,640]{1,0:T(8,128)(2,1)S(1)} %shard_map.153.refs_1_), channel_id=1, source_target_pairs={{0,4},{4,0},{1,5},{5,1},{2,6},{6,2},{3,7},{7,3},{8,12},{12,8},{9,1... | collective-permute-start | bytes 2949128 | tf_op jit(solution)/shard_map/ppermute | solution.py:29
  52.5 11.4 %collective-permute-start.10 = (bf16[256,768]{1,0:T(8,128)(2,1)S(1)}, bf16[256,768]{1,0:T(8,128)(2,1)S(1)}, u32[]{:S(2)}, u32[]{:S(2)}) collective-permute-start(bf16[256,768]{1,0:T(8,128)(2,1)S(1)} %collective-permute-done.9.refs_2_), channel_id=1, source_target_pairs={{0,32},{4,228},{32,64},{36,4},{64,96},{68,36},{96,128},{100,68},{1... | collective-permute-start | bytes 1179656 | tf_op jit(solution)/shard_map/ppermute | solution.py:42
  52.5 10.4 %collective-permute-start.24 = (bf16[256,640]{1,0:T(8,128)(2,1)S(1)}, bf16[256,640]{1,0:T(8,128)(2,1)S(1)}, u32[]{:S(2)}, u32[]{:S(2)}) collective-permute-start(bf16[256,640]{1,0:T(8,128)(2,1)S(1)} %collective-permute-done.23.refs_2_), channel_id=1, source_target_pairs={{0,32},{4,228},{32,64},{36,4},{64,96},{68,36},{96,128},{100,68},{1... | collective-permute-start | bytes 983048 | tf_op jit(solution)/shard_map/ppermute | solution.py:42
  63.0 14.0 %collective-permute-start.26 = (bf16[512,1024]{1,0:T(8,128)(2,1)S(1)}, bf16[512,1024]{1,0:T(8,128)(2,1)S(1)}, u32[]{:S(2)}, u32[]{:S(2)}) collective-permute-start(bf16[512,1024]{1,0:T(8,128)(2,1)S(1)} %shard_map.154.refs_0_), channel_id=1, source_target_pairs={{0,8},{4,28},{8,16},{12,4},{16,24},{20,12},{24,0},{28,20},{1,9},{5... | collective-permute-start | bytes 3145736 | tf_op jit(solution)/shard_map/ppermute | solution.py:42
  63.9 22.4 %collective-permute-start.12 = (bf16[2048,256]{1,0:T(8,128)(2,1)S(1)}, bf16[2048,256]{1,0:T(8,128)(2,1)S(1)}, u32[]{:S(2)}, u32[]{:S(2)}) collective-permute-start(bf16[2048,256]{1,0:T(8,128)(2,1)S(1)} %shard_map.148.refs_0_), channel_id=1, source_target_pairs={{0,1},{4,7},{1,2},{5,4},{2,3},{6,5},{3,0},{7,6},{8,9},{12,15},{9,1... | collective-permute-start | bytes 3145736 | tf_op jit(solution)/shard_map/ppermute | solution.py:42
  66.5 22.4 %collective-permute-start.16 = (bf16[128,2048]{1,0:T(8,128)(2,1)S(1)}, bf16[128,2048]{1,0:T(8,128)(2,1)S(1)}, u32[]{:S(2)}, u32[]{:S(2)}) collective-permute-start(bf16[128,2048]{1,0:T(8,128)(2,1)S(1)} %slice.7), channel_id=1, source_target_pairs={{0,4},{4,8},{8,12},{12,16},{16,20},{20,24},{24,28},{28,32},{32,36}... | collective-permute-start | bytes 1572872 | tf_op jit(solution)/shard_map/ppermute | solution.py:372
  77.0 43.8 %collective-permute-start.27 = (bf16[512,1024]{1,0:T(8,128)(2,1)S(1)}, bf16[512,1024]{1,0:T(8,128)(2,1)S(1)}, u32[]{:S(2)}, u32[]{:S(2)}) collective-permute-start(bf16[512,1024]{1,0:T(8,128)(2,1)S(1)} %collective-permute-done.26.refs_1_), channel_id=1, source_target_pairs={{0,8},{4,28},{8,16},{12,4},{16,24},{20,12},{24,0},{28,20},{1,9},{5... | collective-permute-start | bytes 3145736 | tf_op jit(solution)/shard_map/ppermute | solution.py:42
  79.0 44.3 %collective-permute-start.28 = (bf16[512,1024]{1,0:T(8,128)(2,1)S(1)}, bf16[512,1024]{1,0:T(8,128)(2,1)S(1)}, u32[]{:S(2)}, u32[]{:S(2)}) collective-permute-start(bf16[512,1024]{1,0:T(8,128)(2,1)S(1)} %collective-permute-done.26.refs_1_), channel_id=1, source_target_pairs={{0,4},{4,0},{1,5},{5,1},{2,6},{6,2},{3,7},{7,3},{8,12},{12,8},{9,1... | collective-permute-start | bytes 3145736 | tf_op jit(solution)/shard_map/ppermute | solution.py:29
  86.3 23.7 %collective-permute-start.13 = (bf16[1024,256]{1,0:T(8,128)(2,1)S(1)}, bf16[1024,256]{1,0:T(8,128)(2,1)S(1)}, u32[]{:S(2)}, u32[]{:S(2)}) collective-permute-start(bf16[1024,256]{1,0:T(8,128)(2,1)S(1)} %slice.8), channel_id=1, source_target_pairs={{0,1},{4,7},{1,2},{5,4},{2,3},{6,5},{3,0},{7,6},{8,9},{12,15},{9,1... | collective-permute-start | bytes 1572872 | tf_op jit(solution)/shard_map/ppermute | solution.py:42
  88.9 40.2 %collective-permute-start.14 = (bf16[2048,256]{1,0:T(8,128)(2,1)S(1)}, bf16[2048,256]{1,0:T(8,128)(2,1)S(1)}, u32[]{:S(2)}, u32[]{:S(2)}) collective-permute-start(bf16[2048,256]{1,0:T(8,128)(2,1)S(1)} %collective-permute-done.12.refs_1_), channel_id=1, source_target_pairs={{0,4},{4,0},{1,5},{5,1},{2,6},{6,2},{3,7},{7,3},{8,12},{12,8},{9,1... | collective-permute-start | bytes 3145736 | tf_op jit(solution)/shard_map/ppermute | solution.py:29
  103.5 5.9 %collective-permute-start.29 = (bf16[256,256]{1,0:T(8,128)(2,1)S(1)}, bf16[256,256]{1,0:T(8,128)(2,1)S(1)}, u32[]{:S(2)}, u32[]{:S(2)}) collective-permute-start(bf16[256,256]{1,0:T(8,128)(2,1)S(1)} %get-tuple-element.30), channel_id=1, source_target_pairs={{0,1},{1,2},{2,3},{3,0},{4,5},{5,6},{6,7},{7,4},{8,9},{9,10},{10,1... | collective-permute-start | bytes 393224 | tf_op jit(solution)/shard_map/ppermute | solution.py:89
  109.4 5.3 %collective-permute-start.30 = (bf16[256,256]{1,0:T(8,128)(2,1)S(1)}, bf16[256,256]{1,0:T(8,128)(2,1)S(1)}, u32[]{:S(2)}, u32[]{:S(2)}) collective-permute-start(bf16[256,256]{1,0:T(8,128)(2,1)S(1)} %get-tuple-element.31), channel_id=1, source_target_pairs={{0,2},{1,3},{2,0},{3,1},{4,6},{5,7},{6,4},{7,5},{8,10},{9,11},{10,... | collective-permute-start | bytes 393224 | tf_op jit(solution)/shard_map/ppermute | solution.py:89
  110.1 19.0 %collective-permute-start.15 = (bf16[1024,256]{1,0:T(8,128)(2,1)S(1)}, bf16[1024,256]{1,0:T(8,128)(2,1)S(1)}, u32[]{:S(2)}, u32[]{:S(2)}) collective-permute-start(bf16[1024,256]{1,0:T(8,128)(2,1)S(1)} %collective-permute-done.13.refs_2_), channel_id=1, source_target_pairs={{0,4},{4,0},{1,5},{5,1},{2,6},{6,2},{3,7},{7,3},{8,12},{12,8},{9,1... | collective-permute-start | bytes 1572872 | tf_op jit(solution)/shard_map/ppermute | solution.py:29
  114.7 5.3 %collective-permute-start.31 = (bf16[256,256]{1,0:T(8,128)(2,1)S(1)}, bf16[256,256]{1,0:T(8,128)(2,1)S(1)}, u32[]{:S(2)}, u32[]{:S(2)}) collective-permute-start(bf16[256,256]{1,0:T(8,128)(2,1)S(1)} %get-tuple-element.32), channel_id=1, source_target_pairs={{0,3},{1,0},{2,1},{3,2},{4,7},{5,4},{6,5},{7,6},{8,11},{9,8},{10,9... | collective-permute-start | bytes 393224 | tf_op jit(solution)/shard_map/ppermute | solution.py:89
  120.0 7.1 %collective-permute-start.17 = (bf16[272,256]{1,0:T(8,128)(2,1)S(1)}, bf16[272,256]{1,0:T(8,128)(2,1)S(1)}, u32[]{:S(2)}, u32[]{:S(2)}) collective-permute-start(bf16[272,256]{1,0:T(8,128)(2,1)S(1)} %get-tuple-element.23), channel_id=1, source_target_pairs={{0,1},{1,2},{2,3},{3,0},{4,5},{5,6},{6,7},{7,4},{8,9},{9,10},{10,1... | collective-permute-start | bytes 417800 | tf_op jit(solution)/shard_map/ppermute | solution.py:89
  120.8 8.3 %collective-permute-start.18 = (bf16[272,256]{1,0:T(8,128)(2,1)S(1)}, bf16[272,256]{1,0:T(8,128)(2,1)S(1)}, u32[]{:S(2)}, u32[]{:S(2)}) collective-permute-start(bf16[272,256]{1,0:T(8,128)(2,1)S(1)} %get-tuple-element.24), channel_id=1, source_target_pairs={{0,2},{1,3},{2,0},{3,1},{4,6},{5,7},{6,4},{7,5},{8,10},{9,11},{10,... | collective-permute-start | bytes 417800 | tf_op jit(solution)/shard_map/ppermute | solution.py:89
  123.3 5.8 %collective-permute-start.19 = (bf16[272,256]{1,0:T(8,128)(2,1)S(1)}, bf16[272,256]{1,0:T(8,128)(2,1)S(1)}, u32[]{:S(2)}, u32[]{:S(2)}) collective-permute-start(bf16[272,256]{1,0:T(8,128)(2,1)S(1)} %get-tuple-element.25), channel_id=1, source_target_pairs={{0,3},{1,0},{2,1},{3,2},{4,7},{5,4},{6,5},{7,6},{8,11},{9,8},{10,9... | collective-permute-start | bytes 417800 | tf_op jit(solution)/shard_map/ppermute | solution.py:89
  (9 other events, 58.2 us)
where the time goes:
time: 135 us; the launch traced here: 134 us
  starting transfers between devices  65.1 us (48%)
  waiting for transfers between devices  36.5 us (27%)
  Pallas kernels  30.4 us (23%)
  local copies, waits for them, and re-layouts  1.71 us (1%)
    ppermute x12, starting transfers between devices, onward(): out = lax.ppermute(v, ('c', 'x') if axis == 'x' else (axis, 'c'), route)  26.9 us
    ppermute x12, waiting for transfers between devices, onward(): out = lax.ppermute(v, ('c', 'x') if axis == 'x' else (axis, 'c'), route)  23.5 us
    ppermute x7, starting transfers between devices, to_partner(): out = lax.ppermute(v, 'c', [(0, 1), (1, 0)])  19.5 us
    ppermute x12, starting transfers between devices, shift(): return lax.ppermute(v, axis, [(i, (i + r) % size) for i in range(size)])  15.7 us
    ppermute x12, waiting for transfers between devices, shift(): return lax.ppermute(v, axis, [(i, (i + r) % size) for i in range(size)])  10.5 us
    pallas_call x1, Pallas kernels, shards(): kernel_call(attention_kernel, out_shape=tuple([jax.ShapeDtypeStruct((shar...  7.04 us
    pallas_call x1, Pallas kernels, shards(): kernel_call(functools.partial(out_conv_kernel, tables(conv_parts)), out_s...  4.74 us
    pallas_call x1, Pallas kernels, shards(): kernel_call(conv_kernel, out_shape=tuple([jax.ShapeDtypeStruct((share + 1...  4.57 us
  transfers between devices with their start and end apart: 32, of which 15 were waited for; matrix products, arithmetic and copies ran while one was open for 0% of the time, Pallas kernels for 19%

commit v1 on v0

--- a/solution.py
+++ b/solution.py
@@ -19,6 +19,7 @@
 SP = ("z", "y", "c")
 NX = 4
 F32 = jnp.float32
+UNROLL = 7
 BF16 = jnp.bfloat16
 
 
@@ -137,29 +138,24 @@
     return x * cosine + other * sine
 
 
-def prep_kernel(tokens_ref, prior_ref, gain_ref, scaled_ref, inv_ref):
+def prep_kernel(tokens_ref, gain_ref, scaled_ref, inv_ref):
     def scale(wide, i):
         rows = pl.ds(pl.multiple_of(i * 32, 32), 32)
         scaled_ref[rows, :] = (wide * gain_ref[...]).astype(BF16)
         mean = jnp.sum(wide * wide, axis=1, keepdims=True) * (1.0 / wide.shape[1])
         inv_ref[rows, :] = jnp.broadcast_to(lax.rsqrt(mean + EPS), (32, 128))
 
-    def before(i, _):
-        scale(prior_ref[pl.ds(pl.multiple_of(i * 32, 32), 32), :].astype(F32), i)
-        return 0
-
     def tile(i, _):
-        scale(tokens_ref[pl.ds(pl.multiple_of(i * 32, 32), 32), :].astype(F32), i + WINDOW // 32)
-        return 0
-
-    lax.fori_loop(0, WINDOW // 32, before, 0)
+        scale(tokens_ref[pl.ds(pl.multiple_of(i * 32, 32), 32), :].astype(F32), i)
+        return 0
+
     lax.fori_loop(0, tokens_ref.shape[0] // 32, tile, 0, unroll=2)
 
 
 def rope_tables():
     half = HEAD_DIM // 2
     inverse = np.tile(1.0 / THETA ** (np.arange(half) * 2.0 / HEAD_DIM), 4)[None, :]
-    steps = np.concatenate([np.arange(32), 1024 * np.arange(64), 32 * np.arange(-4, 36)])[:, None]
+    steps = np.concatenate([np.arange(32), 1024 * np.arange(64), 32 * np.arange(40)])[:, None]
     return jnp.asarray(np.cos(steps * inverse), F32), jnp.asarray(np.sin(steps * inverse), F32)
 
 
@@ -173,7 +169,7 @@
     x_ref, inv_ref, cos_ref, sin_ref, q_ref, kv_ref, w_ref = refs[n_pieces:]
     put_rows(table, pieces, w_ref)
     sp = sp_place()
-    size = 384
+    size = 256
 
     def tile(i, _):
         rows = pl.ds(pl.multiple_of(i * size, 128), size)
@@ -206,9 +202,9 @@
 def glu_kernel(table, *refs):
     n_pieces = len(table)
     pieces = refs[:n_pieces]
-    x_ref, inv_ref, glu_ref, w_ref = refs[n_pieces:]
+    x_ref, inv_ref, kv_ref, glu_ref, tail_ref, w_ref = refs[n_pieces:]
     put_rows(table, pieces, w_ref)
-    size = 384
+    size = 256
 
     def tile(i, _):
         rows = pl.ds(pl.multiple_of(i * size, 128), size)
@@ -218,48 +214,81 @@
         return 0
 
     lax.fori_loop(0, x_ref.shape[0] // size, tile, 0)
-
-
-def attention_kernel(sink_ref, q_ref, kv_ref, *refs):
-    block_refs, (k_ref, v_ref, out_ref) = refs[:NX], refs[NX:]
-    tokens = q_ref.shape[0] - WINDOW
-    for half in range(2):
-        for src, dst in ((kv_ref, 0),):
-            rows = src.shape[0]
-            keep = lane_is((rows, 128), 128, 64)
-            if half:
-                keep = jnp.logical_not(keep)
-            zero = jnp.zeros((rows, 128), BF16)
-            k_ref[half, dst : dst + rows, :] = jnp.where(keep, src[:, 0:128], zero)
-            v_ref[half, dst : dst + rows, :] = jnp.where(keep, src[:, 128:256], zero)
-    row = lax.broadcasted_iota(jnp.int32, (128, 256), 0)
-    col = lax.broadcasted_iota(jnp.int32, (128, 256), 1)
-    band = (col > row) & (col <= row + 128)
+    tail_ref[0:WINDOW, :] = kv_ref[kv_ref.shape[0] - WINDOW :, :]
+    tail_ref[WINDOW:, :] = glu_ref[glu_ref.shape[0] - 32 :, :]
+
+
+def half_zero(rows):
+    first = lane_is(rows.shape, 128, 64)
+    zero = jnp.zeros(rows.shape, BF16)
+    return jnp.where(first, rows, zero), jnp.where(first, zero, rows)
+
+
+def attend(q_pair, keys, values, allowed, sink_ref):
+    outs = []
+    for pair in range(2):
+        q = q_pair(pair)
+        total = None
+        for half in range(2):
+            scores = lax.dot_general(q, keys[half], (((1,), (1,)), ((), ())), preferred_element_type=F32)
+            scores = jnp.where(allowed, scores, -1e30)
+            sink = sink_ref[pair * 2 + half]
+            top = jnp.maximum(jnp.max(scores, axis=1, keepdims=True), sink)
+            weights = jnp.exp(scores - top)
+            denominator = jnp.sum(weights, axis=1, keepdims=True) + jnp.exp(sink - top)
+            probability = (weights * (1.0 / denominator)).astype(BF16)
+            part = jnp.dot(probability, values[half], preferred_element_type=F32)
+            total = part if total is None else total + part
+        outs.append(total.astype(BF16))
+    return outs
+
+
+def in_window():
+    query = lax.broadcasted_iota(jnp.int32, (128, 256), 0)
+    key = lax.broadcasted_iota(jnp.int32, (128, 256), 1)
+    return (key > query) & (key <= query + WINDOW), key
+
+
+def attention_kernel(sink_ref, q_ref, kv_ref, out_ref, k_ref, v_ref):
+    k_ref[0], k_ref[1] = half_zero(kv_ref[:, 0:128])
+    v_ref[0], v_ref[1] = half_zero(kv_ref[:, 128:256])
+    allowed, _ = in_window()
 
     def block(b, _):
         at = pl.multiple_of(b * 128, 128)
-        lowest = jnp.where((b == 0) & (sp_place() == 0), WINDOW, 0)
-        allowed = band & (col >= lowest)
-        for pair in range(2):
-            q = q_ref[pl.ds(at + WINDOW, 128), pair * 128 : pair * 128 + 128]
-            total = None
-            for half in range(2):
-                scores = lax.dot_general(
-                    q, k_ref[half, pl.ds(at, 256), :], (((1,), (1,)), ((), ())), preferred_element_type=F32
-                )
-                scores = jnp.where(allowed, scores, -1e30)
-                sink = sink_ref[pair * 2 + half]
-                row_max = jnp.maximum(jnp.max(scores, axis=1, keepdims=True), sink)
-                weights = jnp.exp(scores - row_max)
-                denominator = jnp.sum(weights, axis=1, keepdims=True) + jnp.exp(sink - row_max)
-                probability = (weights * (1.0 / denominator)).astype(BF16)
-                part = jnp.dot(probability, v_ref[half, pl.ds(at, 256), :], preferred_element_type=F32)
-                total = part if total is None else total + part
-            out_ref[pl.ds(at, 128), pair * 128 : pair * 128 + 128] = total.astype(BF16)
-        return 0
-
-    lax.fori_loop(0, tokens // 128, block, 0, unroll=2)
-    to_blocks(out_ref, block_refs)
+        before = pl.multiple_of(b * 128 - 128, 128)
+        outs = attend(
+            lambda pair: q_ref[pl.ds(at, 128), pair * 128 : pair * 128 + 128],
+            [k_ref[half, pl.ds(before, 256), :] for half in range(2)],
+            [v_ref[half, pl.ds(before, 256), :] for half in range(2)],
+            allowed,
+            sink_ref,
+        )
+        for pair, out in enumerate(outs):
+            out_ref[pl.ds(at, 128), pair * 128 : pair * 128 + 128] = out
+        return 0
+
+    lax.fori_loop(1, q_ref.shape[0] // 128, block, 0, unroll=UNROLL)
+
+
+def first_attention_kernel(sink_ref, q_ref, kv_ref, prior_ref, rest_ref, *block_refs):
+    kv = jnp.concatenate([prior_ref[0:WINDOW, :], kv_ref[0:128, :]], 0)
+    allowed, key = in_window()
+    allowed = allowed & (key >= jnp.where(sp_place() == 0, WINDOW, 0))
+    out = attend(
+        lambda pair: q_ref[0:128, pair * 128 : pair * 128 + 128],
+        half_zero(kv[:, 0:128]),
+        half_zero(kv[:, 128:256]),
+        allowed,
+        sink_ref,
+    )
+    to_blocks(rest_ref, block_refs)
+    for r, ref in enumerate(block_refs):
+
+        @pl.when(((lax.axis_index("x") + r) & 3) == 0)
+        def _(ref=ref):
+            for pair in range(2):
+                ref[0:128, pair * 128 : pair * 128 + 128] = out[pair]
 
 
 def to_blocks(src_ref, block_refs):
@@ -269,10 +298,11 @@
         ref[0:share, :] = src_ref[pl.ds(at, share), :]
 
 
-def conv_kernel(glu_ref, w_ref, bias_ref, gain_ref, *refs):
+def conv_kernel(glu_ref, prior_ref, w_ref, bias_ref, gain_ref, *refs):
     block_refs, (shift_ref, out_ref) = refs[:NX], refs[NX:]
-    tokens = glu_ref.shape[0] - WINDOW
-    shift_ref[0, 0 : 32 + tokens, :] = glu_ref[WINDOW - 32 :, :].astype(F32)
+    tokens = glu_ref.shape[0]
+    shift_ref[0, 0:32, :] = prior_ref[WINDOW:, :].astype(F32)
+    shift_ref[0, 32 : 32 + tokens, :] = glu_ref[...].astype(F32)
 
     def fill(i, _):
         at = pl.multiple_of(i * 32, 32)
@@ -369,7 +399,6 @@
     own_in = jnp.concatenate([w_query, w_key, w_value, w_content, w_gate, out_conv.T], 1)
     lines = around_y(own_in, OWN)
     beside = around_x([out_attn.T] * NX)
-    prior = lax.ppermute(tokens[count - WINDOW :], SP, [(i, i + 1) for i in range(63)])
     width_1, width_2 = n_qkv + wide, n_in - n_qkv + wide
     plan = []
     for k in range(4):
@@ -417,56 +446,65 @@
     scaled, inv_rms = kernel_call(
         prep_kernel,
         out_shape=(
-            jax.ShapeDtypeStruct((WINDOW + count, tokens.shape[1]), BF16),
-            jax.ShapeDtypeStruct((WINDOW + count, 128), F32),
+            jax.ShapeDtypeStruct(tokens.shape, BF16),
+            jax.ShapeDtypeStruct((count, 128), F32),
         ),
-        in_specs=vmem(3),
+        in_specs=vmem(2),
         out_specs=tuple(vmem(2)),
         compiler_params=params(4),
         cost_estimate=cost(1 << 30, 8 << 20),
-    )(tokens, prior, norm_gain.reshape(1, -1))
+    )(tokens, norm_gain.reshape(1, -1))
 
     pieces = [v for v, _ in qkv_parts]
     queries, keys_values = kernel_call(
         functools.partial(qkv_kernel, tables(qkv_parts)),
-        out_shape=(jax.ShapeDtypeStruct((WINDOW + count, 256), BF16),) * 2,
+        out_shape=(jax.ShapeDtypeStruct((count, 256), BF16),) * 2,
         in_specs=vmem(len(pieces) + 4),
         out_specs=tuple(vmem(2)),
         scratch_shapes=[pltpu.VMEM((2048, n_qkv), BF16)],
         compiler_params=params(8),
         cost_estimate=cost(2 * count * 2048 * 384, 8 << 20),
     )(*pieces, scaled, inv_rms, *rope_tables())
-    glu = kernel_call(
+    glu, tail = kernel_call(
         functools.partial(glu_kernel, tables(cg_parts)),
-        out_shape=jax.ShapeDtypeStruct((WINDOW + count, 256), BF16),
-        in_specs=vmem(len(cg_parts) + 2),
-        out_specs=vmem(1)[0],
+        out_shape=(jax.ShapeDtypeStruct((count, 256), BF16), jax.ShapeDtypeStruct((WINDOW + 32, 256), BF16)),
+        in_specs=vmem(len(cg_parts) + 3),
+        out_specs=tuple(vmem(2)),
         scratch_shapes=[pltpu.VMEM((2048, n_in - n_qkv), BF16)],
         compiler_params=params(8),
         cost_estimate=cost(2 * count * 2048 * 512, 8 << 20),
-    )(*[v for v, _ in cg_parts], scaled, inv_rms)
+    )(*[v for v, _ in cg_parts], scaled, inv_rms, keys_values)
+    prior = lax.ppermute(tail, SP, [(i, i + 1) for i in range(63)])
 
     share = count // NX
-    attn_blocks = kernel_call(
+    attended = kernel_call(
         attention_kernel,
-        out_shape=tuple([jax.ShapeDtypeStruct((share, 256), BF16)] * NX),
+        out_shape=jax.ShapeDtypeStruct((count, 256), BF16),
         in_specs=[SMEM] + vmem(2),
-        out_specs=tuple(vmem(NX)),
-        scratch_shapes=[pltpu.VMEM((2, WINDOW + count, 128), BF16)] * 2 + [pltpu.VMEM((count, 256), BF16)],
+        out_specs=vmem(1)[0],
+        scratch_shapes=[pltpu.VMEM((2, count, 128), BF16)] * 2,
         compiler_params=params(8),
         cost_estimate=cost(2 * count * 2048 * 512, 8 << 20),
     )(sink_logit, queries, keys_values)
+    attn_blocks = kernel_call(
+        first_attention_kernel,
+        out_shape=tuple([jax.ShapeDtypeStruct((share, 256), BF16)] * NX),
+        in_specs=[SMEM] + vmem(4),
+        out_specs=tuple(vmem(NX)),
+        compiler_params=params(4),
+        cost_estimate=cost(1 << 30, 1 << 20),
+    )(sink_logit, queries, keys_values, prior, attended)
     attn_blocks = around_x(attn_blocks)
 
     conv_blocks = kernel_call(
         conv_kernel,
         out_shape=tuple([jax.ShapeDtypeStruct((share + 16, 256), BF16)] * NX),
-        in_specs=vmem(4),
+        in_specs=vmem(5),
         out_specs=tuple(vmem(NX)),
         scratch_shapes=[pltpu.VMEM((8, count + 48, 256), F32), pltpu.VMEM((count, 256), BF16)],
         compiler_params=params(16),
         cost_estimate=cost(2 * count * 2048 * 512, 8 << 20),
-    )(glu, conv_weight, conv_bias.reshape(1, -1), channel_gain.reshape(1, -1))
+    )(glu, prior, conv_weight, conv_bias.reshape(1, -1), channel_gain.reshape(1, -1))
     conv_blocks = around_x(conv_blocks)
 
     partial_sum = kernel_call(

time: 135 us -> 127 us (0.941)
  the two profiles are of different devices: /device:TPU:1 before, /device:TPU:10 now
where the time goes in v1:
time: 127 us
  waiting for transfers between devices  61.8 us (49%)
  starting transfers between devices  33.9 us (27%)
  Pallas kernels  29.5 us (23%)
  local copies, waits for them, and re-layouts  1.68 us (1%)
    ppermute x12, waiting for transfers between devices, onward(): out = lax.ppermute(v, ('c', 'x') if axis == 'x' else (axis, 'c'), route)  43.6 us
    ppermute x12, starting transfers between devices, shift(): return lax.ppermute(v, axis, [(i, (i + r) % size) for i in range(size)])  19.7 us
    ppermute x12, waiting for transfers between devices, shift(): return lax.ppermute(v, axis, [(i, (i + r) % size) for i in range(size)])  15.8 us
    ppermute x12, starting transfers between devices, onward(): out = lax.ppermute(v, ('c', 'x') if axis == 'x' else (axis, 'c'), route)  7.31 us
    pallas_call x1, Pallas kernels, shards(): kernel_call(attention_kernel, out_shape=jax.ShapeDtypeStruct((count, 256)...  5.56 us
    ppermute x7, starting transfers between devices, to_partner(): out = lax.ppermute(v, 'c', [(0, 1), (1, 0)])  4.9 us
    pallas_call x1, Pallas kernels, shards(): kernel_call(functools.partial(out_conv_kernel, tables(conv_parts)), out_s...  4.74 us
    pallas_call x1, Pallas kernels, shards(): kernel_call(conv_kernel, out_shape=tuple([jax.ShapeDtypeStruct((share + 1...  4.57 us
  transfers between devices with their start and end apart: 32, of which 18 were waited for; matrix products, arithmetic and copies ran while one was open for 0% of the time, Pallas kernels for 19%

profile of v1, /device:TPU:10, one launch (start us, length us, event | category | flops | bytes accessed | tf_op | source)
XLA Modules:
  0.0 127.2 jit_solution(16960039830124653087)
XLA Ops:
  0.9 1.6 %collective-permute-start = (bf16[32,1152]{1,0:T(8,128)(2,1)S(1)}, bf16[32,1152]{1,0:T(8,128)(2,1)S(1)}, u32[]{:S(2)}, u32[]{:S(2)}) collective-permute-start(bf16[32,1152]{1,0:T(8,128)(2,1)S(1)} %concatenate.3.refs_0_), channel_id=1, source_target_pairs={{0,8},{8,16},{16,24},{24,0},{1,9},{9,17},{17,25},{25,1},{2,10},{10... | collective-permute-start | bytes 221192 | tf_op jit(solution)/shard_map/ppermute | solution.py:90
  3.0 2.3 %collective-permute-start.2 = (bf16[32,1152]{1,0:T(8,128)(2,1)S(1)}, bf16[32,1152]{1,0:T(8,128)(2,1)S(1)}, u32[]{:S(2)}, u32[]{:S(2)}) collective-permute-start(bf16[32,1152]{1,0:T(8,128)(2,1)S(1)} %concatenate.3.refs_0_), channel_id=1, source_target_pairs={{0,16},{8,24},{16,0},{24,8},{1,17},{9,25},{17,1},{25,9},{2,18},{10... | collective-permute-start | bytes 221192 | tf_op jit(solution)/shard_map/ppermute | solution.py:90
  9.2 1.7 %collective-permute-start.5 = (bf16[32,256]{1,0:T(8,128)(2,1)}, bf16[32,256]{1,0:T(8,128)(2,1)S(1)}, u32[]{:S(2)}, u32[]{:S(2)}) collective-permute-start(bf16[32,256]{1,0:T(8,128)(2,1)} %bitcast.7), channel_id=1, source_target_pairs={{0,3},{1,0},{2,1},{3,2},{4,7},{5,4},{6,5},{7,6},{8,11},{9,8},{10,9... | collective-permute-start | bytes 49160 | tf_op jit(solution)/shard_map/ppermute | solution.py:90
  15.5 2.0 %collective-permute-start.7 = (bf16[256,768]{1,0:T(8,128)(2,1)S(1)}, bf16[256,768]{1,0:T(8,128)(2,1)S(1)}, u32[]{:S(2)}, u32[]{:S(2)}) collective-permute-start(bf16[256,768]{1,0:T(8,128)(2,1)S(1)} %shard_map.146.refs_0_), channel_id=1, source_target_pairs={{0,32},{4,228},{32,64},{36,4},{64,96},{68,36},{96,128},{100,68},{1... | collective-permute-start | bytes 1179656 | tf_op jit(solution)/shard_map/ppermute | solution.py:43
  17.5 3.8 %collective-permute-start.16 = (bf16[128,640]{1,0:T(8,128)(2,1)S(1)}, bf16[128,640]{1,0:T(8,128)(2,1)S(1)}, u32[]{:S(2)}, u32[]{:S(2)}) collective-permute-start(bf16[128,640]{1,0:T(8,128)(2,1)S(1)} %get-tuple-element.24.refs_0_), channel_id=1, source_target_pairs={{0,4},{4,0},{1,5},{5,1},{2,6},{6,2},{3,7},{7,3},{8,12},{12,8},{9,1... | collective-permute-start | bytes 491528 | tf_op jit(solution)/shard_map/ppermute | solution.py:30
  22.4 4.7 %collective-permute-done.7.refs_0_ = bf16[256,768]{1,0:T(8,128)(2,1)S(1)} collective-permute-done((bf16[256,768]{1,0:T(8,128)(2,1)S(1)}, bf16[256,768]{1,0:T(8,128)(2,1)S(1)}, u32[]{:S(2)}, u32[]{:S(2)}) %collective-permute-start.7) | collective-permute-done | bytes 393248 | tf_op jit(solution)/shard_map/ppermute | solution.py:43
  27.2 3.5 %collective-permute-done.17.refs_0_ = bf16[256,640]{1,0:T(8,128)(2,1)S(1)} collective-permute-done((bf16[256,640]{1,0:T(8,128)(2,1)S(1)}, bf16[256,640]{1,0:T(8,128)(2,1)S(1)}, u32[]{:S(2)}, u32[]{:S(2)}) %collective-permute-start.17) | collective-permute-done | bytes 327712 | tf_op jit(solution)/shard_map/ppermute | solution.py:43
  30.7 5.5 %collective-permute-done.8.refs_1_ = bf16[256,768]{1,0:T(8,128)(2,1)S(1)} collective-permute-done((bf16[256,768]{1,0:T(8,128)(2,1)S(1)}, bf16[256,768]{1,0:T(8,128)(2,1)S(1)}, u32[]{:S(2)}, u32[]{:S(2)}) %collective-permute-start.8) | collective-permute-done | bytes 393248 | tf_op jit(solution)/shard_map/ppermute | solution.py:43
  36.2 3.5 %collective-permute-done.18.refs_1_ = bf16[256,640]{1,0:T(8,128)(2,1)S(1)} collective-permute-done((bf16[256,640]{1,0:T(8,128)(2,1)S(1)}, bf16[256,640]{1,0:T(8,128)(2,1)S(1)}, u32[]{:S(2)}, u32[]{:S(2)}) %collective-permute-start.18) | collective-permute-done | bytes 327712 | tf_op jit(solution)/shard_map/ppermute | solution.py:43
  39.7 5.5 %collective-permute-done.9.refs_2_ = bf16[256,768]{1,0:T(8,128)(2,1)S(1)} collective-permute-done((bf16[256,768]{1,0:T(8,128)(2,1)S(1)}, bf16[256,768]{1,0:T(8,128)(2,1)S(1)}, u32[]{:S(2)}, u32[]{:S(2)}) %collective-permute-start.9) | collective-permute-done | bytes 393248 | tf_op jit(solution)/shard_map/ppermute | solution.py:43
  45.4 3.3 %collective-permute-done.19.refs_2_ = bf16[256,640]{1,0:T(8,128)(2,1)S(1)} collective-permute-done((bf16[256,640]{1,0:T(8,128)(2,1)S(1)}, bf16[256,640]{1,0:T(8,128)(2,1)S(1)}, u32[]{:S(2)}, u32[]{:S(2)}) %collective-permute-start.19) | collective-permute-done | bytes 327712 | tf_op jit(solution)/shard_map/ppermute | solution.py:43
  49.2 8.0 %collective-permute-done.20.refs_2_ = bf16[256,640]{1,0:T(8,128)(2,1)S(1)} collective-permute-done((bf16[256,640]{1,0:T(8,128)(2,1)S(1)}, bf16[256,640]{1,0:T(8,128)(2,1)S(1)}, u32[]{:S(2)}, u32[]{:S(2)}) %collective-permute-start.20) | collective-permute-done | bytes 327712 | tf_op jit(solution)/shard_map/ppermute | solution.py:43
  58.2 3.2 %collective-permute-done.10.refs_2_ = bf16[256,768]{1,0:T(8,128)(2,1)S(1)} collective-permute-done((bf16[256,768]{1,0:T(8,128)(2,1)S(1)}, bf16[256,768]{1,0:T(8,128)(2,1)S(1)}, u32[]{:S(2)}, u32[]{:S(2)}) %collective-permute-start.10) | collective-permute-done | bytes 393248 | tf_op jit(solution)/shard_map/ppermute | solution.py:43
  61.5 1.6 %collective-permute-start.12 = (bf16[2048,256]{1,0:T(8,128)(2,1)S(1)}, bf16[2048,256]{1,0:T(8,128)(2,1)S(1)}, u32[]{:S(2)}, u32[]{:S(2)}) collective-permute-start(bf16[2048,256]{1,0:T(8,128)(2,1)S(1)} %shard_map.148.refs_0_), channel_id=1, source_target_pairs={{0,1},{4,7},{1,2},{5,4},{2,3},{6,5},{3,0},{7,6},{8,9},{12,15},{9,1... | collective-permute-start | bytes 3145736 | tf_op jit(solution)/shard_map/ppermute | solution.py:43
  63.1 2.8 %shard_map.149 = (bf16[1024,2048]{1,0:T(8,128)(2,1)S(1)}, f32[1024,128]{1,0:T(8,128)S(1)}) custom-call(bf16[1024,2048]{1,0:T(8,128)(2,1)S(1)} %copy-done, f32[1,2048]{1,0:T(1,128)S(1)} %bitcast.9), custom_call_target="tpu_custom_call" | custom-call | flops 1073741824 | bytes 8388608 | tf_op jit(solution)/shard_map/pallas_call | solution.py:446
  65.9 6.3 %collective-permute-done.26.refs_1_ = bf16[512,1024]{1,0:T(8,128)(2,1)S(1)} collective-permute-done((bf16[512,1024]{1,0:T(8,128)(2,1)S(1)}, bf16[512,1024]{1,0:T(8,128)(2,1)S(1)}, u32[]{:S(2)}, u32[]{:S(2)}) %collective-permute-start.26) | collective-permute-done | bytes 1048608 | tf_op jit(solution)/shard_map/ppermute | solution.py:43
  73.0 4.0 %shard_map.152 = (bf16[1024,256]{1,0:T(8,128)(2,1)S(1)}, bf16[1024,256]{1,0:T(8,128)(2,1)S(1)}) custom-call(bf16[256,640]{1,0:T(8,128)(2,1)S(1)} %shard_map.150.refs_0_, bf16[768,640]{1,0:T(8,128)(2,1)S(1)} %shard_map.151.refs_1_, bf16[256,640]{1,0:T(8,128)(2,1)S(1)} %collective-permute-done.20.refs_2_, ...), custom_call_target="tpu_custom_call" | custom-call | flops 1610612736 | bytes 8388608 | tf_op jit(solution)/shard_map/pallas_call | solution.py:459
  77.1 1.6 %collective-permute-start.13 = (bf16[1024,256]{1,0:T(8,128)(2,1)S(1)}, bf16[1024,256]{1,0:T(8,128)(2,1)S(1)}, u32[]{:S(2)}, u32[]{:S(2)}) collective-permute-start(bf16[1024,256]{1,0:T(8,128)(2,1)S(1)} %slice.4), channel_id=1, source_target_pairs={{0,1},{4,7},{1,2},{5,4},{2,3},{6,5},{3,0},{7,6},{8,9},{12,15},{9,1... | collective-permute-start | bytes 1572872 | tf_op jit(solution)/shard_map/ppermute | solution.py:43
  79.1 3.0 %shard_map.153 = (bf16[1024,256]{1,0:T(8,128)(2,1)S(1)}, bf16[160,256]{1,0:T(8,128)(2,1)S(1)}) custom-call(bf16[256,768]{1,0:T(8,128)(2,1)S(1)} %shard_map.146.refs_0_, bf16[768,768]{1,0:T(8,128)(2,1)S(1)} %shard_map.147.refs_1_, bf16[256,768]{1,0:T(8,128)(2,1)S(1)} %collective-permute-done.10.refs_2_, bf16[768,768]{1,0:T(8,128)(2,1)S(1)} %collective-permute-done.11.refs_3_, ...), custom_call_target="tpu_custom_call" | custom-call | flops 2147483648 | bytes 8388608 | tf_op jit(solution)/shard_map/pallas_call | solution.py:468
  82.2 2.0 %collective-permute-start.22 = (bf16[160,256]{1,0:T(8,128)(2,1)S(1)}, bf16[160,256]{1,0:T(8,128)(2,1)S(1)}, u32[]{:S(2)}, u32[]{:S(2)}) collective-permute-start(bf16[160,256]{1,0:T(8,128)(2,1)S(1)} %get-tuple-element.27), channel_id=1, source_target_pairs={{0,4},{4,8},{8,12},{12,16},{16,20},{20,24},{24,28},{28,32},{32,36}... | collective-permute-start | bytes 245768 | tf_op jit(solution)/shard_map/ppermute | solution.py:477
  84.2 5.6 %shard_map.156.rest_ref = bf16[1024,256]{1,0:T(8,128)(2,1)S(1)} custom-call(f32[4]{0:T(128)S(1)} %copy-done.8, bf16[1024,256]{1,0:T(8,128)(2,1)S(1)} %get-tuple-element.32.q_ref, bf16[1024,256]{1,0:T(8,128)(2,1)S(1)} %get-tuple-element.25.refs_6_.kv_ref), custom_call_target="tpu_custom_call" | custom-call | flops 2147483648 | bytes 8388608 | tf_op jit(solution)/shard_map/pallas_call | solution.py:480
  91.2 2.5 %collective-permute-start.29 = (bf16[256,256]{1,0:T(8,128)(2,1)S(1)}, bf16[256,256]{1,0:T(8,128)(2,1)S(1)}, u32[]{:S(2)}, u32[]{:S(2)}) collective-permute-start(bf16[256,256]{1,0:T(8,128)(2,1)S(1)} %get-tuple-element.34), channel_id=1, source_target_pairs={{0,1},{1,2},{2,3},{3,0},{4,5},{5,6},{6,7},{7,4},{8,9},{9,10},{10,1... | collective-permute-start | bytes 393224 | tf_op jit(solution)/shard_map/ppermute | solution.py:90
  94.0 4.0 %collective-permute-done.29.refs_5_ = bf16[256,256]{1,0:T(8,128)(2,1)S(1)} collective-permute-done((bf16[256,256]{1,0:T(8,128)(2,1)S(1)}, bf16[256,256]{1,0:T(8,128)(2,1)S(1)}, u32[]{:S(2)}, u32[]{:S(2)}) %collective-permute-start.29) | collective-permute-done | bytes 131104 | tf_op jit(solution)/shard_map/ppermute | solution.py:90
  98.0 2.0 %collective-permute-start.30 = (bf16[256,256]{1,0:T(8,128)(2,1)S(1)}, bf16[256,256]{1,0:T(8,128)(2,1)S(1)}, u32[]{:S(2)}, u32[]{:S(2)}) collective-permute-start(bf16[256,256]{1,0:T(8,128)(2,1)S(1)} %get-tuple-element.35), channel_id=1, source_target_pairs={{0,2},{1,3},{2,0},{3,1},{4,6},{5,7},{6,4},{7,5},{8,10},{9,11},{10,... | collective-permute-start | bytes 393224 | tf_op jit(solution)/shard_map/ppermute | solution.py:90
  100.0 5.1 %collective-permute-done.30.refs_6_ = bf16[256,256]{1,0:T(8,128)(2,1)S(1)} collective-permute-done((bf16[256,256]{1,0:T(8,128)(2,1)S(1)}, bf16[256,256]{1,0:T(8,128)(2,1)S(1)}, u32[]{:S(2)}, u32[]{:S(2)}) %collective-permute-start.30) | collective-permute-done | bytes 131104 | tf_op jit(solution)/shard_map/ppermute | solution.py:90
  105.1 3.5 %collective-permute-start.31 = (bf16[256,256]{1,0:T(8,128)(2,1)S(1)}, bf16[256,256]{1,0:T(8,128)(2,1)S(1)}, u32[]{:S(2)}, u32[]{:S(2)}) collective-permute-start(bf16[256,256]{1,0:T(8,128)(2,1)S(1)} %get-tuple-element.36), channel_id=1, source_target_pairs={{0,3},{1,0},{2,1},{3,2},{4,7},{5,4},{6,5},{7,6},{8,11},{9,8},{10,9... | collective-permute-start | bytes 393224 | tf_op jit(solution)/shard_map/ppermute | solution.py:90
  108.6 4.6 %shard_map.154 = (bf16[272,256]{1,0:T(8,128)(2,1)S(1)}, bf16[272,256]{1,0:T(8,128)(2,1)S(1)}, bf16[272,256]{1,0:T(8,128)(2,1)S(1)}, bf16[272,256]{1,0:T(8,128)(2,1)S(1)}) custom-call(bf16[1024,256]{1,0:T(8,128)(2,1)S(1)} %get-tuple-element.26.glu_ref, bf16[160,256]{1,0:T(8,128)(2,1)S(1)} %collective-permute-done.22.prior_ref, f32[31,256]{1,0:T(8,128)S(1)} %copy-done.5, ...), custom_call_target="tpu_custom_call" | custom-call | flops 2147483648 | bytes 8388608 | tf_op jit(solution)/shard_map/pallas_call | solution.py:499
  113.3 2.3 %collective-permute-start.24 = (bf16[272,256]{1,0:T(8,128)(2,1)S(1)}, bf16[272,256]{1,0:T(8,128)(2,1)S(1)}, u32[]{:S(2)}, u32[]{:S(2)}) collective-permute-start(bf16[272,256]{1,0:T(8,128)(2,1)S(1)} %get-tuple-element.30), channel_id=1, source_target_pairs={{0,2},{1,3},{2,0},{3,1},{4,6},{5,7},{6,4},{7,5},{8,10},{9,11},{10,... | collective-permute-start | bytes 417800 | tf_op jit(solution)/shard_map/ppermute | solution.py:90
  116.2 3.1 %shard_map.158.refs_9_ = f32[256,2048]{1,0:T(8,128)S(1)} custom-call(bf16[512,1024]{1,0:T(8,128)(2,1)S(1)} %shard_map.155.refs_0_, bf16[512,1024]{1,0:T(8,128)(2,1)S(1)} %collective-permute-done.26.refs_1_, bf16[512,1024]{1,0:T(8,128)(2,1)S(1)} %collective-permute-done.27.refs_2_, bf16[512,1024]{1,0:T(8,128)(2,1)S(1)} %collective-permute-done.28.refs_3_, ...), custom_call_target="tpu_custom_call" | custom-call | flops 1073741824 | bytes 6291456 | tf_op jit(solution)/shard_map/pallas_call | solution.py:510
  119.3 1.6 %collective-permute-done.24.refs_7_ = bf16[272,256]{1,0:T(8,128)(2,1)S(1)} collective-permute-done((bf16[272,256]{1,0:T(8,128)(2,1)S(1)}, bf16[272,256]{1,0:T(8,128)(2,1)S(1)}, u32[]{:S(2)}, u32[]{:S(2)}) %collective-permute-start.24) | collective-permute-done | bytes 139296 | tf_op jit(solution)/shard_map/ppermute | solution.py:90
  120.9 1.5 %collective-permute-done.25.refs_8_ = bf16[272,256]{1,0:T(8,128)(2,1)S(1)} collective-permute-done((bf16[272,256]{1,0:T(8,128)(2,1)S(1)}, bf16[272,256]{1,0:T(8,128)(2,1)S(1)}, u32[]{:S(2)}, u32[]{:S(2)}) %collective-permute-start.25) | collective-permute-done | bytes 139296 | tf_op jit(solution)/shard_map/ppermute | solution.py:90
  122.4 4.7 %shard_map.159 = bf16[256,2048]{1,0:T(8,128)(2,1)} custom-call(bf16[2048,256]{1,0:T(8,128)(2,1)S(1)} %shard_map.148.refs_0_, bf16[2048,256]{1,0:T(8,128)(2,1)S(1)} %collective-permute-done.12.refs_1_, bf16[1024,256]{1,0:T(8,128)(2,1)S(1)} %collective-permute-done.13.refs_2_, bf16[2048,256]{1,0:T(8,128)(2,1)S(1)} %collective-permute-done.14.refs_3_, ...), custom_call_target="tpu_custom_call" | custom-call | flops 1073741824 | bytes 6291456 | tf_op jit(solution)/shard_map/pallas_call | solution.py:519
  (67 shorter events, 16.5 us)
Async XLA Ops:
  0.9 12.3 %collective-permute-start = (bf16[32,1152]{1,0:T(8,128)(2,1)S(1)}, bf16[32,1152]{1,0:T(8,128)(2,1)S(1)}, u32[]{:S(2)}, u32[]{:S(2)}) collective-permute-start(bf16[32,1152]{1,0:T(8,128)(2,1)S(1)} %concatenate.3.refs_0_), channel_id=1, source_target_pairs={{0,8},{8,16},{16,24},{24,0},{1,9},{9,17},{17,25},{25,1},{2,10},{10... | collective-permute-start | bytes 221192 | tf_op jit(solution)/shard_map/ppermute | solution.py:90
  2.5 10.7 %collective-permute-start.1 = (bf16[32,1152]{1,0:T(8,128)(2,1)S(1)}, bf16[32,1152]{1,0:T(8,128)(2,1)S(1)}, u32[]{:S(2)}, u32[]{:S(2)}) collective-permute-start(bf16[32,1152]{1,0:T(8,128)(2,1)S(1)} %concatenate.3.refs_0_), channel_id=1, source_target_pairs={{0,24},{8,0},{16,8},{24,16},{1,25},{9,1},{17,9},{25,17},{2,26},{10... | collective-permute-start | bytes 221192 | tf_op jit(solution)/shard_map/ppermute | solution.py:90
  3.0 10.2 %collective-permute-start.2 = (bf16[32,1152]{1,0:T(8,128)(2,1)S(1)}, bf16[32,1152]{1,0:T(8,128)(2,1)S(1)}, u32[]{:S(2)}, u32[]{:S(2)}) collective-permute-start(bf16[32,1152]{1,0:T(8,128)(2,1)S(1)} %concatenate.3.refs_0_), channel_id=1, source_target_pairs={{0,16},{8,24},{16,0},{24,8},{1,17},{9,25},{17,1},{25,9},{2,18},{10... | collective-permute-start | bytes 221192 | tf_op jit(solution)/shard_map/ppermute | solution.py:90
  5.3 3.9 %collective-permute-start.3 = (bf16[32,256]{1,0:T(8,128)(2,1)}, bf16[32,256]{1,0:T(8,128)(2,1)S(1)}, u32[]{:S(2)}, u32[]{:S(2)}) collective-permute-start(bf16[32,256]{1,0:T(8,128)(2,1)} %bitcast.5), channel_id=1, source_target_pairs={{0,1},{1,2},{2,3},{3,0},{4,5},{5,6},{6,7},{7,4},{8,9},{9,10},{10,1... | collective-permute-start | bytes 49160 | tf_op jit(solution)/shard_map/ppermute | solution.py:90
  6.8 5.5 %collective-permute-start.4 = (bf16[32,256]{1,0:T(8,128)(2,1)}, bf16[32,256]{1,0:T(8,128)(2,1)S(1)}, u32[]{:S(2)}, u32[]{:S(2)}) collective-permute-start(bf16[32,256]{1,0:T(8,128)(2,1)} %bitcast.6), channel_id=1, source_target_pairs={{0,2},{1,3},{2,0},{3,1},{4,6},{5,7},{6,4},{7,5},{8,10},{9,11},{10,... | collective-permute-start | bytes 49160 | tf_op jit(solution)/shard_map/ppermute | solution.py:90
  9.2 3.9 %collective-permute-start.5 = (bf16[32,256]{1,0:T(8,128)(2,1)}, bf16[32,256]{1,0:T(8,128)(2,1)S(1)}, u32[]{:S(2)}, u32[]{:S(2)}) collective-permute-start(bf16[32,256]{1,0:T(8,128)(2,1)} %bitcast.7), channel_id=1, source_target_pairs={{0,3},{1,0},{2,1},{3,2},{4,7},{5,4},{6,5},{7,6},{8,11},{9,8},{10,9... | collective-permute-start | bytes 49160 | tf_op jit(solution)/shard_map/ppermute | solution.py:90
  13.9 1.5 %collective-permute-start.6 = (bf16[128,768]{1,0:T(8,128)(2,1)S(1)}, bf16[128,768]{1,0:T(8,128)(2,1)S(1)}, u32[]{:S(2)}, u32[]{:S(2)}) collective-permute-start(bf16[128,768]{1,0:T(8,128)(2,1)S(1)} %get-tuple-element.21.refs_0_), channel_id=1, source_target_pairs={{0,4},{4,0},{1,5},{5,1},{2,6},{6,2},{3,7},{7,3},{8,12},{12,8},{9,1... | collective-permute-start | bytes 589832 | tf_op jit(solution)/shard_map/ppermute | solution.py:30
  15.5 11.7 %collective-permute-start.7 = (bf16[256,768]{1,0:T(8,128)(2,1)S(1)}, bf16[256,768]{1,0:T(8,128)(2,1)S(1)}, u32[]{:S(2)}, u32[]{:S(2)}) collective-permute-start(bf16[256,768]{1,0:T(8,128)(2,1)S(1)} %shard_map.146.refs_0_), channel_id=1, source_target_pairs={{0,32},{4,228},{32,64},{36,4},{64,96},{68,36},{96,128},{100,68},{1... | collective-permute-start | bytes 1179656 | tf_op jit(solution)/shard_map/ppermute | solution.py:43
  17.5 4.8 %collective-permute-start.16 = (bf16[128,640]{1,0:T(8,128)(2,1)S(1)}, bf16[128,640]{1,0:T(8,128)(2,1)S(1)}, u32[]{:S(2)}, u32[]{:S(2)}) collective-permute-start(bf16[128,640]{1,0:T(8,128)(2,1)S(1)} %get-tuple-element.24.refs_0_), channel_id=1, source_target_pairs={{0,4},{4,0},{1,5},{5,1},{2,6},{6,2},{3,7},{7,3},{8,12},{12,8},{9,1... | collective-permute-start | bytes 491528 | tf_op jit(solution)/shard_map/ppermute | solution.py:30
  22.4 8.4 %collective-permute-start.17 = (bf16[256,640]{1,0:T(8,128)(2,1)S(1)}, bf16[256,640]{1,0:T(8,128)(2,1)S(1)}, u32[]{:S(2)}, u32[]{:S(2)}) collective-permute-start(bf16[256,640]{1,0:T(8,128)(2,1)S(1)} %shard_map.150.refs_0_), channel_id=1, source_target_pairs={{0,32},{4,228},{32,64},{36,4},{64,96},{68,36},{96,128},{100,68},{1... | collective-permute-start | bytes 983048 | tf_op jit(solution)/shard_map/ppermute | solution.py:43
  27.2 9.0 %collective-permute-start.8 = (bf16[256,768]{1,0:T(8,128)(2,1)S(1)}, bf16[256,768]{1,0:T(8,128)(2,1)S(1)}, u32[]{:S(2)}, u32[]{:S(2)}) collective-permute-start(bf16[256,768]{1,0:T(8,128)(2,1)S(1)} %collective-permute-done.7.refs_0_), channel_id=1, source_target_pairs={{0,32},{4,228},{32,64},{36,4},{64,96},{68,36},{96,128},{100,68},{1... | collective-permute-start | bytes 1179656 | tf_op jit(solution)/shard_map/ppermute | solution.py:43
  30.7 9.0 %collective-permute-start.18 = (bf16[256,640]{1,0:T(8,128)(2,1)S(1)}, bf16[256,640]{1,0:T(8,128)(2,1)S(1)}, u32[]{:S(2)}, u32[]{:S(2)}) collective-permute-start(bf16[256,640]{1,0:T(8,128)(2,1)S(1)} %collective-permute-done.17.refs_0_), channel_id=1, source_target_pairs={{0,32},{4,228},{32,64},{36,4},{64,96},{68,36},{96,128},{100,68},{1... | collective-permute-start | bytes 983048 | tf_op jit(solution)/shard_map/ppermute | solution.py:43
  36.2 9.0 %collective-permute-start.9 = (bf16[256,768]{1,0:T(8,128)(2,1)S(1)}, bf16[256,768]{1,0:T(8,128)(2,1)S(1)}, u32[]{:S(2)}, u32[]{:S(2)}) collective-permute-start(bf16[256,768]{1,0:T(8,128)(2,1)S(1)} %collective-permute-done.8.refs_1_), channel_id=1, source_target_pairs={{0,32},{4,228},{32,64},{36,4},{64,96},{68,36},{96,128},{100,68},{1... | collective-permute-start | bytes 1179656 | tf_op jit(solution)/shard_map/ppermute | solution.py:43
  39.7 9.0 %collective-permute-start.19 = (bf16[256,640]{1,0:T(8,128)(2,1)S(1)}, bf16[256,640]{1,0:T(8,128)(2,1)S(1)}, u32[]{:S(2)}, u32[]{:S(2)}) collective-permute-start(bf16[256,640]{1,0:T(8,128)(2,1)S(1)} %collective-permute-done.18.refs_1_), channel_id=1, source_target_pairs={{0,32},{4,228},{32,64},{36,4},{64,96},{68,36},{96,128},{100,68},{1... | collective-permute-start | bytes 983048 | tf_op jit(solution)/shard_map/ppermute | solution.py:43
  45.3 16.2 %collective-permute-start.11 = (bf16[768,768]{1,0:T(8,128)(2,1)S(1)}, bf16[768,768]{1,0:T(8,128)(2,1)S(1)}, u32[]{:S(2)}, u32[]{:S(2)}) collective-permute-start(bf16[768,768]{1,0:T(8,128)(2,1)S(1)} %shard_map.147.refs_1_), channel_id=1, source_target_pairs={{0,4},{4,0},{1,5},{5,1},{2,6},{6,2},{3,7},{7,3},{8,12},{12,8},{9,1... | collective-permute-start | bytes 3538952 | tf_op jit(solution)/shard_map/ppermute | solution.py:30
  48.8 8.5 %collective-permute-start.21 = (bf16[768,640]{1,0:T(8,128)(2,1)S(1)}, bf16[768,640]{1,0:T(8,128)(2,1)S(1)}, u32[]{:S(2)}, u32[]{:S(2)}) collective-permute-start(bf16[768,640]{1,0:T(8,128)(2,1)S(1)} %shard_map.151.refs_1_), channel_id=1, source_target_pairs={{0,4},{4,0},{1,5},{5,1},{2,6},{6,2},{3,7},{7,3},{8,12},{12,8},{9,1... | collective-permute-start | bytes 2949128 | tf_op jit(solution)/shard_map/ppermute | solution.py:30
  48.9 8.4 %collective-permute-start.20 = (bf16[256,640]{1,0:T(8,128)(2,1)S(1)}, bf16[256,640]{1,0:T(8,128)(2,1)S(1)}, u32[]{:S(2)}, u32[]{:S(2)}) collective-permute-start(bf16[256,640]{1,0:T(8,128)(2,1)S(1)} %collective-permute-done.19.refs_2_), channel_id=1, source_target_pairs={{0,32},{4,228},{32,64},{36,4},{64,96},{68,36},{96,128},{100,68},{1... | collective-permute-start | bytes 983048 | tf_op jit(solution)/shard_map/ppermute | solution.py:43
  49.0 12.5 %collective-permute-start.10 = (bf16[256,768]{1,0:T(8,128)(2,1)S(1)}, bf16[256,768]{1,0:T(8,128)(2,1)S(1)}, u32[]{:S(2)}, u32[]{:S(2)}) collective-permute-start(bf16[256,768]{1,0:T(8,128)(2,1)S(1)} %collective-permute-done.9.refs_2_), channel_id=1, source_target_pairs={{0,32},{4,228},{32,64},{36,4},{64,96},{68,36},{96,128},{100,68},{1... | collective-permute-start | bytes 1179656 | tf_op jit(solution)/shard_map/ppermute | solution.py:43
  57.3 14.9 %collective-permute-start.26 = (bf16[512,1024]{1,0:T(8,128)(2,1)S(1)}, bf16[512,1024]{1,0:T(8,128)(2,1)S(1)}, u32[]{:S(2)}, u32[]{:S(2)}) collective-permute-start(bf16[512,1024]{1,0:T(8,128)(2,1)S(1)} %shard_map.155.refs_0_), channel_id=1, source_target_pairs={{0,8},{4,28},{8,16},{12,4},{16,24},{20,12},{24,0},{28,20},{1,9},{5... | collective-permute-start | bytes 3145736 | tf_op jit(solution)/shard_map/ppermute | solution.py:43
  61.5 15.5 %collective-permute-start.12 = (bf16[2048,256]{1,0:T(8,128)(2,1)S(1)}, bf16[2048,256]{1,0:T(8,128)(2,1)S(1)}, u32[]{:S(2)}, u32[]{:S(2)}) collective-permute-start(bf16[2048,256]{1,0:T(8,128)(2,1)S(1)} %shard_map.148.refs_0_), channel_id=1, source_target_pairs={{0,1},{4,7},{1,2},{5,4},{2,3},{6,5},{3,0},{7,6},{8,9},{12,15},{9,1... | collective-permute-start | bytes 3145736 | tf_op jit(solution)/shard_map/ppermute | solution.py:43
  72.2 41.1 %collective-permute-start.27 = (bf16[512,1024]{1,0:T(8,128)(2,1)S(1)}, bf16[512,1024]{1,0:T(8,128)(2,1)S(1)}, u32[]{:S(2)}, u32[]{:S(2)}) collective-permute-start(bf16[512,1024]{1,0:T(8,128)(2,1)S(1)} %collective-permute-done.26.refs_1_), channel_id=1, source_target_pairs={{0,8},{4,28},{8,16},{12,4},{16,24},{20,12},{24,0},{28,20},{1,9},{5... | collective-permute-start | bytes 3145736 | tf_op jit(solution)/shard_map/ppermute | solution.py:43
  73.0 42.6 %collective-permute-start.28 = (bf16[512,1024]{1,0:T(8,128)(2,1)S(1)}, bf16[512,1024]{1,0:T(8,128)(2,1)S(1)}, u32[]{:S(2)}, u32[]{:S(2)}) collective-permute-start(bf16[512,1024]{1,0:T(8,128)(2,1)S(1)} %collective-permute-done.26.refs_1_), channel_id=1, source_target_pairs={{0,4},{4,0},{1,5},{5,1},{2,6},{6,2},{3,7},{7,3},{8,12},{12,8},{9,1... | collective-permute-start | bytes 3145736 | tf_op jit(solution)/shard_map/ppermute | solution.py:30
  77.1 16.5 %collective-permute-start.13 = (bf16[1024,256]{1,0:T(8,128)(2,1)S(1)}, bf16[1024,256]{1,0:T(8,128)(2,1)S(1)}, u32[]{:S(2)}, u32[]{:S(2)}) collective-permute-start(bf16[1024,256]{1,0:T(8,128)(2,1)S(1)} %slice.4), channel_id=1, source_target_pairs={{0,1},{4,7},{1,2},{5,4},{2,3},{6,5},{3,0},{7,6},{8,9},{12,15},{9,1... | collective-permute-start | bytes 1572872 | tf_op jit(solution)/shard_map/ppermute | solution.py:43
  78.7 43.7 %collective-permute-start.14 = (bf16[2048,256]{1,0:T(8,128)(2,1)S(1)}, bf16[2048,256]{1,0:T(8,128)(2,1)S(1)}, u32[]{:S(2)}, u32[]{:S(2)}) collective-permute-start(bf16[2048,256]{1,0:T(8,128)(2,1)S(1)} %collective-permute-done.12.refs_1_), channel_id=1, source_target_pairs={{0,4},{4,0},{1,5},{5,1},{2,6},{6,2},{3,7},{7,3},{8,12},{12,8},{9,1... | collective-permute-start | bytes 3145736 | tf_op jit(solution)/shard_map/ppermute | solution.py:30
  82.2 7.6 %collective-permute-start.22 = (bf16[160,256]{1,0:T(8,128)(2,1)S(1)}, bf16[160,256]{1,0:T(8,128)(2,1)S(1)}, u32[]{:S(2)}, u32[]{:S(2)}) collective-permute-start(bf16[160,256]{1,0:T(8,128)(2,1)S(1)} %get-tuple-element.27), channel_id=1, source_target_pairs={{0,4},{4,8},{8,12},{12,16},{16,20},{20,24},{24,28},{28,32},{32,36}... | collective-permute-start | bytes 245768 | tf_op jit(solution)/shard_map/ppermute | solution.py:477
  91.2 6.9 %collective-permute-start.29 = (bf16[256,256]{1,0:T(8,128)(2,1)S(1)}, bf16[256,256]{1,0:T(8,128)(2,1)S(1)}, u32[]{:S(2)}, u32[]{:S(2)}) collective-permute-start(bf16[256,256]{1,0:T(8,128)(2,1)S(1)} %get-tuple-element.34), channel_id=1, source_target_pairs={{0,1},{1,2},{2,3},{3,0},{4,5},{5,6},{6,7},{7,4},{8,9},{9,10},{10,1... | collective-permute-start | bytes 393224 | tf_op jit(solution)/shard_map/ppermute | solution.py:90
  93.6 28.8 %collective-permute-start.15 = (bf16[1024,256]{1,0:T(8,128)(2,1)S(1)}, bf16[1024,256]{1,0:T(8,128)(2,1)S(1)}, u32[]{:S(2)}, u32[]{:S(2)}) collective-permute-start(bf16[1024,256]{1,0:T(8,128)(2,1)S(1)} %collective-permute-done.13.refs_2_), channel_id=1, source_target_pairs={{0,4},{4,0},{1,5},{5,1},{2,6},{6,2},{3,7},{7,3},{8,12},{12,8},{9,1... | collective-permute-start | bytes 1572872 | tf_op jit(solution)/shard_map/ppermute | solution.py:30
  98.0 7.0 %collective-permute-start.30 = (bf16[256,256]{1,0:T(8,128)(2,1)S(1)}, bf16[256,256]{1,0:T(8,128)(2,1)S(1)}, u32[]{:S(2)}, u32[]{:S(2)}) collective-permute-start(bf16[256,256]{1,0:T(8,128)(2,1)S(1)} %get-tuple-element.35), channel_id=1, source_target_pairs={{0,2},{1,3},{2,0},{3,1},{4,6},{5,7},{6,4},{7,5},{8,10},{9,11},{10,... | collective-permute-start | bytes 393224 | tf_op jit(solution)/shard_map/ppermute | solution.py:90
  105.1 8.1 %collective-permute-start.31 = (bf16[256,256]{1,0:T(8,128)(2,1)S(1)}, bf16[256,256]{1,0:T(8,128)(2,1)S(1)}, u32[]{:S(2)}, u32[]{:S(2)}) collective-permute-start(bf16[256,256]{1,0:T(8,128)(2,1)S(1)} %get-tuple-element.36), channel_id=1, source_target_pairs={{0,3},{1,0},{2,1},{3,2},{4,7},{5,4},{6,5},{7,6},{8,11},{9,8},{10,9... | collective-permute-start | bytes 393224 | tf_op jit(solution)/shard_map/ppermute | solution.py:90
  113.2 6.1 %collective-permute-start.23 = (bf16[272,256]{1,0:T(8,128)(2,1)S(1)}, bf16[272,256]{1,0:T(8,128)(2,1)S(1)}, u32[]{:S(2)}, u32[]{:S(2)}) collective-permute-start(bf16[272,256]{1,0:T(8,128)(2,1)S(1)} %get-tuple-element.29), channel_id=1, source_target_pairs={{0,1},{1,2},{2,3},{3,0},{4,5},{5,6},{6,7},{7,4},{8,9},{9,10},{10,1... | collective-permute-start | bytes 417800 | tf_op jit(solution)/shard_map/ppermute | solution.py:90
  113.3 7.6 %collective-permute-start.24 = (bf16[272,256]{1,0:T(8,128)(2,1)S(1)}, bf16[272,256]{1,0:T(8,128)(2,1)S(1)}, u32[]{:S(2)}, u32[]{:S(2)}) collective-permute-start(bf16[272,256]{1,0:T(8,128)(2,1)S(1)} %get-tuple-element.30), channel_id=1, source_target_pairs={{0,2},{1,3},{2,0},{3,1},{4,6},{5,7},{6,4},{7,5},{8,10},{9,11},{10,... | collective-permute-start | bytes 417800 | tf_op jit(solution)/shard_map/ppermute | solution.py:90
  115.6 6.8 %collective-permute-start.25 = (bf16[272,256]{1,0:T(8,128)(2,1)S(1)}, bf16[272,256]{1,0:T(8,128)(2,1)S(1)}, u32[]{:S(2)}, u32[]{:S(2)}) collective-permute-start(bf16[272,256]{1,0:T(8,128)(2,1)S(1)} %get-tuple-element.31), channel_id=1, source_target_pairs={{0,3},{1,0},{2,1},{3,2},{4,7},{5,4},{6,5},{7,6},{8,11},{9,8},{10,9... | collective-permute-start | bytes 417800 | tf_op jit(solution)/shard_map/ppermute | solution.py:90
  (9 other events, 93.8 us)

commit v2 on v1

--- a/solution.py
+++ b/solution.py
@@ -169,7 +169,7 @@
     x_ref, inv_ref, cos_ref, sin_ref, q_ref, kv_ref, w_ref = refs[n_pieces:]
     put_rows(table, pieces, w_ref)
     sp = sp_place()
-    size = 256
+    size = 1024
 
     def tile(i, _):
         rows = pl.ds(pl.multiple_of(i * size, 128), size)
@@ -204,7 +204,7 @@
     pieces = refs[:n_pieces]
     x_ref, inv_ref, kv_ref, glu_ref, tail_ref, w_ref = refs[n_pieces:]
     put_rows(table, pieces, w_ref)
-    size = 256
+    size = 1024
 
     def tile(i, _):
         rows = pl.ds(pl.multiple_of(i * size, 128), size)
@@ -311,7 +311,7 @@
             shift_ref[b, pl.ds(at, 32), :] = rows[b : b + 32, :]
         return 0
 
-    lax.fori_loop(0, tokens // 32 + 1, fill, 0)
+    lax.fori_loop(0, tokens // 32 + 1, fill, 0, unroll=3)
 
     def tile(i, _):
         at = pl.multiple_of(i * 32, 32)
@@ -323,7 +323,7 @@
         out_ref[pl.ds(at, 32), :] = total.astype(BF16)
         return 0
 
-    lax.fori_loop(0, tokens // 32, tile, 0)
+    lax.fori_loop(0, tokens // 32, tile, 0, unroll=4)
     to_blocks(out_ref, block_refs)
     edge = jnp.concatenate([bias_ref[...], gain_ref[...]], 0)
     high = edge.astype(BF16).astype(F32)
@@ -344,13 +344,13 @@
         act_ref[:, r * wide : (r + 1) * wide] = attn[r][...]
 
     def tile(i, _):
-        at = pl.multiple_of(i * 256, 256)
-        out_ref[:, pl.ds(at, 256)] = lax.dot_general(
-            act_ref[...], w_ref[pl.ds(at, 256), :], (((1,), (1,)), ((), ())), preferred_element_type=F32
+        at = pl.multiple_of(i * 1024, 1024)
+        out_ref[:, pl.ds(at, 1024)] = lax.dot_general(
+            act_ref[...], w_ref[pl.ds(at, 1024), :], (((1,), (1,)), ((), ())), preferred_element_type=F32
         )
         return 0
 
-    lax.fori_loop(0, out_ref.shape[1] // 256, tile, 0)
+    lax.fori_loop(0, out_ref.shape[1] // 1024, tile, 0)
 
 
 def out_conv_kernel(table, *refs):
@@ -373,14 +373,14 @@
         act_ref[:, r * wide : (r + 1) * wide] = (value * jax.nn.sigmoid(value)).astype(BF16)
 
     def tile(i, _):
-        at = pl.multiple_of(i * 256, 256)
+        at = pl.multiple_of(i * 1024, 1024)
         out = lax.dot_general(
-            act_ref[...], w_ref[pl.ds(at, 256), :], (((1,), (1,)), ((), ())), preferred_element_type=F32
+            act_ref[...], w_ref[pl.ds(at, 1024), :], (((1,), (1,)), ((), ())), preferred_element_type=F32
         )
-        out_ref[:, pl.ds(at, 256)] = (out + partial_ref[:, pl.ds(at, 256)]).astype(BF16)
-        return 0
-
-    lax.fori_loop(0, out_ref.shape[1] // 256, tile, 0)
+        out_ref[:, pl.ds(at, 1024)] = (out + partial_ref[:, pl.ds(at, 1024)]).astype(BF16)
+        return 0
+
+    lax.fori_loop(0, out_ref.shape[1] // 1024, tile, 0)
 
 
 def cost(flops, moved):

time: 127 us -> 125 us (0.984)
  the two profiles are of different devices: /device:TPU:10 before, /device:TPU:16 now
where the time goes in v2:
time: 125 us
  waiting for transfers between devices  67.6 us (54%)
  starting transfers between devices  29.9 us (24%)
  Pallas kernels  25 us (20%)
  local copies, waits for them, and re-layouts  1.67 us (1%)
    ppermute x12, waiting for transfers between devices, onward(): out = lax.ppermute(v, ('c', 'x') if axis == 'x' else (axis, 'c'), route)  45.8 us
    ppermute x12, waiting for transfers between devices, shift(): return lax.ppermute(v, axis, [(i, (i + r) % size) for i in range(size)])  19.3 us
    ppermute x12, starting transfers between devices, shift(): return lax.ppermute(v, axis, [(i, (i + r) % size) for i in range(size)])  15.1 us
    ppermute x7, starting transfers between devices, to_partner(): out = lax.ppermute(v, 'c', [(0, 1), (1, 0)])  9.45 us
    pallas_call x1, Pallas kernels, shards(): kernel_call(attention_kernel, out_shape=jax.ShapeDtypeStruct((count, 256)...  5.55 us
    pallas_call x1, Pallas kernels, shards(): kernel_call(conv_kernel, out_shape=tuple([jax.ShapeDtypeStruct((share + 1...  3.9 us
    pallas_call x1, Pallas kernels, shards(): kernel_call(functools.partial(out_conv_kernel, tables(conv_parts)), out_s...  3.49 us
    pallas_call x1, Pallas kernels, shards(): kernel_call(functools.partial(qkv_kernel, tables(qkv_parts)), out_shape=(...  3.24 us
  transfers between devices with their start and end apart: 32, of which 20 were waited for; matrix products, arithmetic and copies ran while one was open for 0% of the time, Pallas kernels for 17%

profile of v2, /device:TPU:16, one launch (start us, length us, event | category | flops | bytes accessed | tf_op | source)
XLA Modules:
  0.0 124.5 jit_solution(5346120137842356783)
XLA Ops:
  3.0 3.3 %collective-permute-start.2 = (bf16[32,1152]{1,0:T(8,128)(2,1)S(1)}, bf16[32,1152]{1,0:T(8,128)(2,1)S(1)}, u32[]{:S(2)}, u32[]{:S(2)}) collective-permute-start(bf16[32,1152]{1,0:T(8,128)(2,1)S(1)} %concatenate.3.refs_0_), channel_id=1, source_target_pairs={{0,16},{8,24},{16,0},{24,8},{1,17},{9,25},{17,1},{25,9},{2,18},{10... | collective-permute-start | bytes 221192 | tf_op jit(solution)/shard_map/ppermute | solution.py:90
  6.2 2.5 %collective-permute-start.4 = (bf16[32,256]{1,0:T(8,128)(2,1)}, bf16[32,256]{1,0:T(8,128)(2,1)S(1)}, u32[]{:S(2)}, u32[]{:S(2)}) collective-permute-start(bf16[32,256]{1,0:T(8,128)(2,1)} %bitcast.6), channel_id=1, source_target_pairs={{0,2},{1,3},{2,0},{3,1},{4,6},{5,7},{6,4},{7,5},{8,10},{9,11},{10,... | collective-permute-start | bytes 49160 | tf_op jit(solution)/shard_map/ppermute | solution.py:90
  8.8 2.6 %collective-permute-done.3.refs_5_ = bf16[32,256]{1,0:T(8,128)(2,1)S(1)} collective-permute-done((bf16[32,256]{1,0:T(8,128)(2,1)}, bf16[32,256]{1,0:T(8,128)(2,1)S(1)}, u32[]{:S(2)}, u32[]{:S(2)}) %collective-permute-start.3) | collective-permute-done | bytes 16416 | tf_op jit(solution)/shard_map/ppermute | solution.py:90
  11.7 3.7 %collective-permute-done.5.refs_7_ = bf16[32,256]{1,0:T(8,128)(2,1)S(1)} collective-permute-done((bf16[32,256]{1,0:T(8,128)(2,1)}, bf16[32,256]{1,0:T(8,128)(2,1)S(1)}, u32[]{:S(2)}, u32[]{:S(2)}) %collective-permute-start.5) | collective-permute-done | bytes 16416 | tf_op jit(solution)/shard_map/ppermute | solution.py:90
  16.2 1.4 %collective-permute-done.6.refs_1_ = bf16[128,768]{1,0:T(8,128)(2,1)S(1)} collective-permute-done((bf16[128,768]{1,0:T(8,128)(2,1)S(1)}, bf16[128,768]{1,0:T(8,128)(2,1)S(1)}, u32[]{:S(2)}, u32[]{:S(2)}) %collective-permute-start.6) | collective-permute-done | bytes 196640 | tf_op jit(solution)/shard_map/ppermute | solution.py:30
  18.0 3.8 %collective-permute-start.16 = (bf16[128,640]{1,0:T(8,128)(2,1)S(1)}, bf16[128,640]{1,0:T(8,128)(2,1)S(1)}, u32[]{:S(2)}, u32[]{:S(2)}) collective-permute-start(bf16[128,640]{1,0:T(8,128)(2,1)S(1)} %get-tuple-element.24.refs_0_), channel_id=1, source_target_pairs={{0,4},{4,0},{1,5},{5,1},{2,6},{6,2},{3,7},{7,3},{8,12},{12,8},{9,1... | collective-permute-start | bytes 491528 | tf_op jit(solution)/shard_map/ppermute | solution.py:30
  22.9 4.7 %collective-permute-done.7.refs_0_ = bf16[256,768]{1,0:T(8,128)(2,1)S(1)} collective-permute-done((bf16[256,768]{1,0:T(8,128)(2,1)S(1)}, bf16[256,768]{1,0:T(8,128)(2,1)S(1)}, u32[]{:S(2)}, u32[]{:S(2)}) %collective-permute-start.7) | collective-permute-done | bytes 393248 | tf_op jit(solution)/shard_map/ppermute | solution.py:43
  27.7 3.5 %collective-permute-done.17.refs_0_ = bf16[256,640]{1,0:T(8,128)(2,1)S(1)} collective-permute-done((bf16[256,640]{1,0:T(8,128)(2,1)S(1)}, bf16[256,640]{1,0:T(8,128)(2,1)S(1)}, u32[]{:S(2)}, u32[]{:S(2)}) %collective-permute-start.17) | collective-permute-done | bytes 327712 | tf_op jit(solution)/shard_map/ppermute | solution.py:43
  31.2 5.5 %collective-permute-done.8.refs_1_ = bf16[256,768]{1,0:T(8,128)(2,1)S(1)} collective-permute-done((bf16[256,768]{1,0:T(8,128)(2,1)S(1)}, bf16[256,768]{1,0:T(8,128)(2,1)S(1)}, u32[]{:S(2)}, u32[]{:S(2)}) %collective-permute-start.8) | collective-permute-done | bytes 393248 | tf_op jit(solution)/shard_map/ppermute | solution.py:43
  36.6 3.5 %collective-permute-done.18.refs_1_ = bf16[256,640]{1,0:T(8,128)(2,1)S(1)} collective-permute-done((bf16[256,640]{1,0:T(8,128)(2,1)S(1)}, bf16[256,640]{1,0:T(8,128)(2,1)S(1)}, u32[]{:S(2)}, u32[]{:S(2)}) %collective-permute-start.18) | collective-permute-done | bytes 327712 | tf_op jit(solution)/shard_map/ppermute | solution.py:43
  40.2 5.5 %collective-permute-done.9.refs_2_ = bf16[256,768]{1,0:T(8,128)(2,1)S(1)} collective-permute-done((bf16[256,768]{1,0:T(8,128)(2,1)S(1)}, bf16[256,768]{1,0:T(8,128)(2,1)S(1)}, u32[]{:S(2)}, u32[]{:S(2)}) %collective-permute-start.9) | collective-permute-done | bytes 393248 | tf_op jit(solution)/shard_map/ppermute | solution.py:43
  45.8 3.3 %collective-permute-done.19.refs_2_ = bf16[256,640]{1,0:T(8,128)(2,1)S(1)} collective-permute-done((bf16[256,640]{1,0:T(8,128)(2,1)S(1)}, bf16[256,640]{1,0:T(8,128)(2,1)S(1)}, u32[]{:S(2)}, u32[]{:S(2)}) %collective-permute-start.19) | collective-permute-done | bytes 327712 | tf_op jit(solution)/shard_map/ppermute | solution.py:43
  49.7 8.0 %collective-permute-done.20.refs_2_ = bf16[256,640]{1,0:T(8,128)(2,1)S(1)} collective-permute-done((bf16[256,640]{1,0:T(8,128)(2,1)S(1)}, bf16[256,640]{1,0:T(8,128)(2,1)S(1)}, u32[]{:S(2)}, u32[]{:S(2)}) %collective-permute-start.20) | collective-permute-done | bytes 327712 | tf_op jit(solution)/shard_map/ppermute | solution.py:43
  58.8 3.1 %collective-permute-done.10.refs_2_ = bf16[256,768]{1,0:T(8,128)(2,1)S(1)} collective-permute-done((bf16[256,768]{1,0:T(8,128)(2,1)S(1)}, bf16[256,768]{1,0:T(8,128)(2,1)S(1)}, u32[]{:S(2)}, u32[]{:S(2)}) %collective-permute-start.10) | collective-permute-done | bytes 393248 | tf_op jit(solution)/shard_map/ppermute | solution.py:43
  62.4 2.8 %shard_map.149 = (bf16[1024,2048]{1,0:T(8,128)(2,1)S(1)}, f32[1024,128]{1,0:T(8,128)S(1)}) custom-call(bf16[1024,2048]{1,0:T(8,128)(2,1)S(1)} %copy-done, f32[1,2048]{1,0:T(1,128)S(1)} %bitcast.9), custom_call_target="tpu_custom_call" | custom-call | flops 1073741824 | bytes 8388608 | tf_op jit(solution)/shard_map/pallas_call | solution.py:446
  65.1 7.5 %collective-permute-done.26.refs_1_ = bf16[512,1024]{1,0:T(8,128)(2,1)S(1)} collective-permute-done((bf16[512,1024]{1,0:T(8,128)(2,1)S(1)}, bf16[512,1024]{1,0:T(8,128)(2,1)S(1)}, u32[]{:S(2)}, u32[]{:S(2)}) %collective-permute-start.26) | collective-permute-done | bytes 1048608 | tf_op jit(solution)/shard_map/ppermute | solution.py:43
  73.6 3.2 %shard_map.152 = (bf16[1024,256]{1,0:T(8,128)(2,1)S(1)}, bf16[1024,256]{1,0:T(8,128)(2,1)S(1)}) custom-call(bf16[256,640]{1,0:T(8,128)(2,1)S(1)} %shard_map.150.refs_0_, bf16[768,640]{1,0:T(8,128)(2,1)S(1)} %shard_map.151.refs_1_, bf16[256,640]{1,0:T(8,128)(2,1)S(1)} %collective-permute-done.20.refs_2_, ...), custom_call_target="tpu_custom_call" | custom-call | flops 1610612736 | bytes 8388608 | tf_op jit(solution)/shard_map/pallas_call | solution.py:459
  78.2 1.8 %collective-permute-start.14 = (bf16[2048,256]{1,0:T(8,128)(2,1)S(1)}, bf16[2048,256]{1,0:T(8,128)(2,1)S(1)}, u32[]{:S(2)}, u32[]{:S(2)}) collective-permute-start(bf16[2048,256]{1,0:T(8,128)(2,1)S(1)} %collective-permute-done.12.refs_1_), channel_id=1, source_target_pairs={{0,4},{4,0},{1,5},{5,1},{2,6},{6,2},{3,7},{7,3},{8,12},{12,8},{9,1... | collective-permute-start | bytes 3145736 | tf_op jit(solution)/shard_map/ppermute | solution.py:30
  80.0 2.5 %shard_map.153 = (bf16[1024,256]{1,0:T(8,128)(2,1)S(1)}, bf16[160,256]{1,0:T(8,128)(2,1)S(1)}) custom-call(bf16[256,768]{1,0:T(8,128)(2,1)S(1)} %shard_map.146.refs_0_, bf16[768,768]{1,0:T(8,128)(2,1)S(1)} %shard_map.147.refs_1_, bf16[256,768]{1,0:T(8,128)(2,1)S(1)} %collective-permute-done.10.refs_2_, bf16[768,768]{1,0:T(8,128)(2,1)S(1)} %collective-permute-done.11.refs_3_, ...), custom_call_target="tpu_custom_call" | custom-call | flops 2147483648 | bytes 8388608 | tf_op jit(solution)/shard_map/pallas_call | solution.py:468
  82.5 2.1 %collective-permute-start.22 = (bf16[160,256]{1,0:T(8,128)(2,1)S(1)}, bf16[160,256]{1,0:T(8,128)(2,1)S(1)}, u32[]{:S(2)}, u32[]{:S(2)}) collective-permute-start(bf16[160,256]{1,0:T(8,128)(2,1)S(1)} %get-tuple-element.27), channel_id=1, source_target_pairs={{0,4},{4,8},{8,12},{12,16},{16,20},{20,24},{24,28},{28,32},{32,36}... | collective-permute-start | bytes 245768 | tf_op jit(solution)/shard_map/ppermute | solution.py:477
  84.6 5.5 %shard_map.156.rest_ref = bf16[1024,256]{1,0:T(8,128)(2,1)S(1)} custom-call(f32[4]{0:T(128)S(1)} %copy-done.8, bf16[1024,256]{1,0:T(8,128)(2,1)S(1)} %get-tuple-element.32.q_ref, bf16[1024,256]{1,0:T(8,128)(2,1)S(1)} %get-tuple-element.25.refs_6_.kv_ref), custom_call_target="tpu_custom_call" | custom-call | flops 2147483648 | bytes 8388608 | tf_op jit(solution)/shard_map/pallas_call | solution.py:480
  90.2 1.4 %shard_map.157 = (bf16[256,256]{1,0:T(8,128)(2,1)S(1)}, bf16[256,256]{1,0:T(8,128)(2,1)S(1)}, bf16[256,256]{1,0:T(8,128)(2,1)S(1)}, bf16[256,256]{1,0:T(8,128)(2,1)S(1)}) custom-call(f32[4]{0:T(128)S(1)} %copy-done.8, bf16[1024,256]{1,0:T(8,128)(2,1)S(1)} %get-tuple-element.32.q_ref, bf16[1024,256]{1,0:T(8,128)(2,1)S(1)} %get-tuple-element.25.refs_6_.kv_ref, ...), custom_call_target="tpu_custom_call" | custom-call | flops 1073741824 | bytes 1048576 | tf_op jit(solution)/shard_map/pallas_call | solution.py:489
  91.8 3.6 %collective-permute-start.15 = (bf16[1024,256]{1,0:T(8,128)(2,1)S(1)}, bf16[1024,256]{1,0:T(8,128)(2,1)S(1)}, u32[]{:S(2)}, u32[]{:S(2)}) collective-permute-start(bf16[1024,256]{1,0:T(8,128)(2,1)S(1)} %collective-permute-done.13.refs_2_), channel_id=1, source_target_pairs={{0,4},{4,0},{1,5},{5,1},{2,6},{6,2},{3,7},{7,3},{8,12},{12,8},{9,1... | collective-permute-start | bytes 1572872 | tf_op jit(solution)/shard_map/ppermute | solution.py:30
  95.3 2.6 %collective-permute-done.29.refs_5_ = bf16[256,256]{1,0:T(8,128)(2,1)S(1)} collective-permute-done((bf16[256,256]{1,0:T(8,128)(2,1)S(1)}, bf16[256,256]{1,0:T(8,128)(2,1)S(1)}, u32[]{:S(2)}, u32[]{:S(2)}) %collective-permute-start.29) | collective-permute-done | bytes 131104 | tf_op jit(solution)/shard_map/ppermute | solution.py:90
  98.5 6.0 %collective-permute-done.30.refs_6_ = bf16[256,256]{1,0:T(8,128)(2,1)S(1)} collective-permute-done((bf16[256,256]{1,0:T(8,128)(2,1)S(1)}, bf16[256,256]{1,0:T(8,128)(2,1)S(1)}, u32[]{:S(2)}, u32[]{:S(2)}) %collective-permute-start.30) | collective-permute-done | bytes 131104 | tf_op jit(solution)/shard_map/ppermute | solution.py:90
  104.4 2.4 %collective-permute-start.31 = (bf16[256,256]{1,0:T(8,128)(2,1)S(1)}, bf16[256,256]{1,0:T(8,128)(2,1)S(1)}, u32[]{:S(2)}, u32[]{:S(2)}) collective-permute-start(bf16[256,256]{1,0:T(8,128)(2,1)S(1)} %get-tuple-element.36), channel_id=1, source_target_pairs={{0,3},{1,0},{2,1},{3,2},{4,7},{5,4},{6,5},{7,6},{8,11},{9,8},{10,9... | collective-permute-start | bytes 393224 | tf_op jit(solution)/shard_map/ppermute | solution.py:90
  106.8 3.9 %shard_map.154 = (bf16[272,256]{1,0:T(8,128)(2,1)S(1)}, bf16[272,256]{1,0:T(8,128)(2,1)S(1)}, bf16[272,256]{1,0:T(8,128)(2,1)S(1)}, bf16[272,256]{1,0:T(8,128)(2,1)S(1)}) custom-call(bf16[1024,256]{1,0:T(8,128)(2,1)S(1)} %get-tuple-element.26.glu_ref, bf16[160,256]{1,0:T(8,128)(2,1)S(1)} %collective-permute-done.22.prior_ref, f32[31,256]{1,0:T(8,128)S(1)} %copy-done.5, ...), custom_call_target="tpu_custom_call" | custom-call | flops 2147483648 | bytes 8388608 | tf_op jit(solution)/shard_map/pallas_call | solution.py:499
  110.8 4.2 %collective-permute-start.24 = (bf16[272,256]{1,0:T(8,128)(2,1)S(1)}, bf16[272,256]{1,0:T(8,128)(2,1)S(1)}, u32[]{:S(2)}, u32[]{:S(2)}) collective-permute-start(bf16[272,256]{1,0:T(8,128)(2,1)S(1)} %get-tuple-element.30), channel_id=1, source_target_pairs={{0,2},{1,3},{2,0},{3,1},{4,6},{5,7},{6,4},{7,5},{8,10},{9,11},{10,... | collective-permute-start | bytes 417800 | tf_op jit(solution)/shard_map/ppermute | solution.py:90
  115.0 1.8 %shard_map.158.refs_9_ = f32[256,2048]{1,0:T(8,128)S(1)} custom-call(bf16[512,1024]{1,0:T(8,128)(2,1)S(1)} %shard_map.155.refs_0_, bf16[512,1024]{1,0:T(8,128)(2,1)S(1)} %collective-permute-done.26.refs_1_, bf16[512,1024]{1,0:T(8,128)(2,1)S(1)} %collective-permute-done.27.refs_2_, bf16[512,1024]{1,0:T(8,128)(2,1)S(1)} %collective-permute-done.28.refs_3_, ...), custom_call_target="tpu_custom_call" | custom-call | flops 1073741824 | bytes 6291456 | tf_op jit(solution)/shard_map/pallas_call | solution.py:510
  116.8 2.0 %collective-permute-done.23.refs_6_ = bf16[272,256]{1,0:T(8,128)(2,1)S(1)} collective-permute-done((bf16[272,256]{1,0:T(8,128)(2,1)S(1)}, bf16[272,256]{1,0:T(8,128)(2,1)S(1)}, u32[]{:S(2)}, u32[]{:S(2)}) %collective-permute-start.23) | collective-permute-done | bytes 139296 | tf_op jit(solution)/shard_map/ppermute | solution.py:90
  118.8 1.9 %collective-permute-done.24.refs_7_ = bf16[272,256]{1,0:T(8,128)(2,1)S(1)} collective-permute-done((bf16[272,256]{1,0:T(8,128)(2,1)S(1)}, bf16[272,256]{1,0:T(8,128)(2,1)S(1)}, u32[]{:S(2)}, u32[]{:S(2)}) %collective-permute-start.24) | collective-permute-done | bytes 139296 | tf_op jit(solution)/shard_map/ppermute | solution.py:90
  121.0 3.5 %shard_map.159 = bf16[256,2048]{1,0:T(8,128)(2,1)} custom-call(bf16[2048,256]{1,0:T(8,128)(2,1)S(1)} %shard_map.148.refs_0_, bf16[2048,256]{1,0:T(8,128)(2,1)S(1)} %collective-permute-done.12.refs_1_, bf16[1024,256]{1,0:T(8,128)(2,1)S(1)} %collective-permute-done.13.refs_2_, bf16[2048,256]{1,0:T(8,128)(2,1)S(1)} %collective-permute-done.14.refs_3_, ...), custom_call_target="tpu_custom_call" | custom-call | flops 1073741824 | bytes 6291456 | tf_op jit(solution)/shard_map/pallas_call | solution.py:519
  (67 shorter events, 11.1 us)
Async XLA Ops:
  0.9 14.5 %collective-permute-start = (bf16[32,1152]{1,0:T(8,128)(2,1)S(1)}, bf16[32,1152]{1,0:T(8,128)(2,1)S(1)}, u32[]{:S(2)}, u32[]{:S(2)}) collective-permute-start(bf16[32,1152]{1,0:T(8,128)(2,1)S(1)} %concatenate.3.refs_0_), channel_id=1, source_target_pairs={{0,8},{8,16},{16,24},{24,0},{1,9},{9,17},{17,25},{25,1},{2,10},{10... | collective-permute-start | bytes 221192 | tf_op jit(solution)/shard_map/ppermute | solution.py:90
  2.2 13.1 %collective-permute-start.1 = (bf16[32,1152]{1,0:T(8,128)(2,1)S(1)}, bf16[32,1152]{1,0:T(8,128)(2,1)S(1)}, u32[]{:S(2)}, u32[]{:S(2)}) collective-permute-start(bf16[32,1152]{1,0:T(8,128)(2,1)S(1)} %concatenate.3.refs_0_), channel_id=1, source_target_pairs={{0,24},{8,0},{16,8},{24,16},{1,25},{9,1},{17,9},{25,17},{2,26},{10... | collective-permute-start | bytes 221192 | tf_op jit(solution)/shard_map/ppermute | solution.py:90
  3.0 12.4 %collective-permute-start.2 = (bf16[32,1152]{1,0:T(8,128)(2,1)S(1)}, bf16[32,1152]{1,0:T(8,128)(2,1)S(1)}, u32[]{:S(2)}, u32[]{:S(2)}) collective-permute-start(bf16[32,1152]{1,0:T(8,128)(2,1)S(1)} %concatenate.3.refs_0_), channel_id=1, source_target_pairs={{0,16},{8,24},{16,0},{24,8},{1,17},{9,25},{17,1},{25,9},{2,18},{10... | collective-permute-start | bytes 221192 | tf_op jit(solution)/shard_map/ppermute | solution.py:90
  6.2 5.2 %collective-permute-start.3 = (bf16[32,256]{1,0:T(8,128)(2,1)}, bf16[32,256]{1,0:T(8,128)(2,1)S(1)}, u32[]{:S(2)}, u32[]{:S(2)}) collective-permute-start(bf16[32,256]{1,0:T(8,128)(2,1)} %bitcast.5), channel_id=1, source_target_pairs={{0,1},{1,2},{2,3},{3,0},{4,5},{5,6},{6,7},{7,4},{8,9},{9,10},{10,1... | collective-permute-start | bytes 49160 | tf_op jit(solution)/shard_map/ppermute | solution.py:90
  6.2 5.5 %collective-permute-start.4 = (bf16[32,256]{1,0:T(8,128)(2,1)}, bf16[32,256]{1,0:T(8,128)(2,1)S(1)}, u32[]{:S(2)}, u32[]{:S(2)}) collective-permute-start(bf16[32,256]{1,0:T(8,128)(2,1)} %bitcast.6), channel_id=1, source_target_pairs={{0,2},{1,3},{2,0},{3,1},{4,6},{5,7},{6,4},{7,5},{8,10},{9,11},{10,... | collective-permute-start | bytes 49160 | tf_op jit(solution)/shard_map/ppermute | solution.py:90
  11.4 3.9 %collective-permute-start.5 = (bf16[32,256]{1,0:T(8,128)(2,1)}, bf16[32,256]{1,0:T(8,128)(2,1)S(1)}, u32[]{:S(2)}, u32[]{:S(2)}) collective-permute-start(bf16[32,256]{1,0:T(8,128)(2,1)} %bitcast.7), channel_id=1, source_target_pairs={{0,3},{1,0},{2,1},{3,2},{4,7},{5,4},{6,5},{7,6},{8,11},{9,8},{10,9... | collective-permute-start | bytes 49160 | tf_op jit(solution)/shard_map/ppermute | solution.py:90
  16.1 1.5 %collective-permute-start.6 = (bf16[128,768]{1,0:T(8,128)(2,1)S(1)}, bf16[128,768]{1,0:T(8,128)(2,1)S(1)}, u32[]{:S(2)}, u32[]{:S(2)}) collective-permute-start(bf16[128,768]{1,0:T(8,128)(2,1)S(1)} %get-tuple-element.21.refs_0_), channel_id=1, source_target_pairs={{0,4},{4,0},{1,5},{5,1},{2,6},{6,2},{3,7},{7,3},{8,12},{12,8},{9,1... | collective-permute-start | bytes 589832 | tf_op jit(solution)/shard_map/ppermute | solution.py:30
  17.7 10.0 %collective-permute-start.7 = (bf16[256,768]{1,0:T(8,128)(2,1)S(1)}, bf16[256,768]{1,0:T(8,128)(2,1)S(1)}, u32[]{:S(2)}, u32[]{:S(2)}) collective-permute-start(bf16[256,768]{1,0:T(8,128)(2,1)S(1)} %shard_map.146.refs_0_), channel_id=1, source_target_pairs={{0,32},{4,228},{32,64},{36,4},{64,96},{68,36},{96,128},{100,68},{1... | collective-permute-start | bytes 1179656 | tf_op jit(solution)/shard_map/ppermute | solution.py:43
  18.0 4.8 %collective-permute-start.16 = (bf16[128,640]{1,0:T(8,128)(2,1)S(1)}, bf16[128,640]{1,0:T(8,128)(2,1)S(1)}, u32[]{:S(2)}, u32[]{:S(2)}) collective-permute-start(bf16[128,640]{1,0:T(8,128)(2,1)S(1)} %get-tuple-element.24.refs_0_), channel_id=1, source_target_pairs={{0,4},{4,0},{1,5},{5,1},{2,6},{6,2},{3,7},{7,3},{8,12},{12,8},{9,1... | collective-permute-start | bytes 491528 | tf_op jit(solution)/shard_map/ppermute | solution.py:30
  22.8 8.4 %collective-permute-start.17 = (bf16[256,640]{1,0:T(8,128)(2,1)S(1)}, bf16[256,640]{1,0:T(8,128)(2,1)S(1)}, u32[]{:S(2)}, u32[]{:S(2)}) collective-permute-start(bf16[256,640]{1,0:T(8,128)(2,1)S(1)} %shard_map.150.refs_0_), channel_id=1, source_target_pairs={{0,32},{4,228},{32,64},{36,4},{64,96},{68,36},{96,128},{100,68},{1... | collective-permute-start | bytes 983048 | tf_op jit(solution)/shard_map/ppermute | solution.py:43
  27.7 9.0 %collective-permute-start.8 = (bf16[256,768]{1,0:T(8,128)(2,1)S(1)}, bf16[256,768]{1,0:T(8,128)(2,1)S(1)}, u32[]{:S(2)}, u32[]{:S(2)}) collective-permute-start(bf16[256,768]{1,0:T(8,128)(2,1)S(1)} %collective-permute-done.7.refs_0_), channel_id=1, source_target_pairs={{0,32},{4,228},{32,64},{36,4},{64,96},{68,36},{96,128},{100,68},{1... | collective-permute-start | bytes 1179656 | tf_op jit(solution)/shard_map/ppermute | solution.py:43
  31.2 9.0 %collective-permute-start.18 = (bf16[256,640]{1,0:T(8,128)(2,1)S(1)}, bf16[256,640]{1,0:T(8,128)(2,1)S(1)}, u32[]{:S(2)}, u32[]{:S(2)}) collective-permute-start(bf16[256,640]{1,0:T(8,128)(2,1)S(1)} %collective-permute-done.17.refs_0_), channel_id=1, source_target_pairs={{0,32},{4,228},{32,64},{36,4},{64,96},{68,36},{96,128},{100,68},{1... | collective-permute-start | bytes 983048 | tf_op jit(solution)/shard_map/ppermute | solution.py:43
  36.6 9.0 %collective-permute-start.9 = (bf16[256,768]{1,0:T(8,128)(2,1)S(1)}, bf16[256,768]{1,0:T(8,128)(2,1)S(1)}, u32[]{:S(2)}, u32[]{:S(2)}) collective-permute-start(bf16[256,768]{1,0:T(8,128)(2,1)S(1)} %collective-permute-done.8.refs_1_), channel_id=1, source_target_pairs={{0,32},{4,228},{32,64},{36,4},{64,96},{68,36},{96,128},{100,68},{1... | collective-permute-start | bytes 1179656 | tf_op jit(solution)/shard_map/ppermute | solution.py:43
  40.2 9.0 %collective-permute-start.19 = (bf16[256,640]{1,0:T(8,128)(2,1)S(1)}, bf16[256,640]{1,0:T(8,128)(2,1)S(1)}, u32[]{:S(2)}, u32[]{:S(2)}) collective-permute-start(bf16[256,640]{1,0:T(8,128)(2,1)S(1)} %collective-permute-done.18.refs_1_), channel_id=1, source_target_pairs={{0,32},{4,228},{32,64},{36,4},{64,96},{68,36},{96,128},{100,68},{1... | collective-permute-start | bytes 983048 | tf_op jit(solution)/shard_map/ppermute | solution.py:43
  45.7 16.2 %collective-permute-start.11 = (bf16[768,768]{1,0:T(8,128)(2,1)S(1)}, bf16[768,768]{1,0:T(8,128)(2,1)S(1)}, u32[]{:S(2)}, u32[]{:S(2)}) collective-permute-start(bf16[768,768]{1,0:T(8,128)(2,1)S(1)} %shard_map.147.refs_1_), channel_id=1, source_target_pairs={{0,4},{4,0},{1,5},{5,1},{2,6},{6,2},{3,7},{7,3},{8,12},{12,8},{9,1... | collective-permute-start | bytes 3538952 | tf_op jit(solution)/shard_map/ppermute | solution.py:30
  49.2 8.5 %collective-permute-start.21 = (bf16[768,640]{1,0:T(8,128)(2,1)S(1)}, bf16[768,640]{1,0:T(8,128)(2,1)S(1)}, u32[]{:S(2)}, u32[]{:S(2)}) collective-permute-start(bf16[768,640]{1,0:T(8,128)(2,1)S(1)} %shard_map.151.refs_1_), channel_id=1, source_target_pairs={{0,4},{4,0},{1,5},{5,1},{2,6},{6,2},{3,7},{7,3},{8,12},{12,8},{9,1... | collective-permute-start | bytes 2949128 | tf_op jit(solution)/shard_map/ppermute | solution.py:30
  49.3 8.4 %collective-permute-start.20 = (bf16[256,640]{1,0:T(8,128)(2,1)S(1)}, bf16[256,640]{1,0:T(8,128)(2,1)S(1)}, u32[]{:S(2)}, u32[]{:S(2)}) collective-permute-start(bf16[256,640]{1,0:T(8,128)(2,1)S(1)} %collective-permute-done.19.refs_2_), channel_id=1, source_target_pairs={{0,32},{4,228},{32,64},{36,4},{64,96},{68,36},{96,128},{100,68},{1... | collective-permute-start | bytes 983048 | tf_op jit(solution)/shard_map/ppermute | solution.py:43
  49.4 12.5 %collective-permute-start.10 = (bf16[256,768]{1,0:T(8,128)(2,1)S(1)}, bf16[256,768]{1,0:T(8,128)(2,1)S(1)}, u32[]{:S(2)}, u32[]{:S(2)}) collective-permute-start(bf16[256,768]{1,0:T(8,128)(2,1)S(1)} %collective-permute-done.9.refs_2_), channel_id=1, source_target_pairs={{0,32},{4,228},{32,64},{36,4},{64,96},{68,36},{96,128},{100,68},{1... | collective-permute-start | bytes 1179656 | tf_op jit(solution)/shard_map/ppermute | solution.py:43
  57.8 14.9 %collective-permute-start.26 = (bf16[512,1024]{1,0:T(8,128)(2,1)S(1)}, bf16[512,1024]{1,0:T(8,128)(2,1)S(1)}, u32[]{:S(2)}, u32[]{:S(2)}) collective-permute-start(bf16[512,1024]{1,0:T(8,128)(2,1)S(1)} %shard_map.155.refs_0_), channel_id=1, source_target_pairs={{0,8},{4,28},{8,16},{12,4},{16,24},{20,12},{24,0},{28,20},{1,9},{5... | collective-permute-start | bytes 3145736 | tf_op jit(solution)/shard_map/ppermute | solution.py:43
  62.0 16.1 %collective-permute-start.12 = (bf16[2048,256]{1,0:T(8,128)(2,1)S(1)}, bf16[2048,256]{1,0:T(8,128)(2,1)S(1)}, u32[]{:S(2)}, u32[]{:S(2)}) collective-permute-start(bf16[2048,256]{1,0:T(8,128)(2,1)S(1)} %shard_map.148.refs_0_), channel_id=1, source_target_pairs={{0,1},{4,7},{1,2},{5,4},{2,3},{6,5},{3,0},{7,6},{8,9},{12,15},{9,1... | collective-permute-start | bytes 3145736 | tf_op jit(solution)/shard_map/ppermute | solution.py:43
  72.7 38.1 %collective-permute-start.27 = (bf16[512,1024]{1,0:T(8,128)(2,1)S(1)}, bf16[512,1024]{1,0:T(8,128)(2,1)S(1)}, u32[]{:S(2)}, u32[]{:S(2)}) collective-permute-start(bf16[512,1024]{1,0:T(8,128)(2,1)S(1)} %collective-permute-done.26.refs_1_), channel_id=1, source_target_pairs={{0,8},{4,28},{8,16},{12,4},{16,24},{20,12},{24,0},{28,20},{1,9},{5... | collective-permute-start | bytes 3145736 | tf_op jit(solution)/shard_map/ppermute | solution.py:43
  73.6 41.4 %collective-permute-start.28 = (bf16[512,1024]{1,0:T(8,128)(2,1)S(1)}, bf16[512,1024]{1,0:T(8,128)(2,1)S(1)}, u32[]{:S(2)}, u32[]{:S(2)}) collective-permute-start(bf16[512,1024]{1,0:T(8,128)(2,1)S(1)} %collective-permute-done.26.refs_1_), channel_id=1, source_target_pairs={{0,4},{4,0},{1,5},{5,1},{2,6},{6,2},{3,7},{7,3},{8,12},{12,8},{9,1... | collective-permute-start | bytes 3145736 | tf_op jit(solution)/shard_map/ppermute | solution.py:30
  78.1 13.6 %collective-permute-start.13 = (bf16[1024,256]{1,0:T(8,128)(2,1)S(1)}, bf16[1024,256]{1,0:T(8,128)(2,1)S(1)}, u32[]{:S(2)}, u32[]{:S(2)}) collective-permute-start(bf16[1024,256]{1,0:T(8,128)(2,1)S(1)} %slice.4), channel_id=1, source_target_pairs={{0,1},{4,7},{1,2},{5,4},{2,3},{6,5},{3,0},{7,6},{8,9},{12,15},{9,1... | collective-permute-start | bytes 1572872 | tf_op jit(solution)/shard_map/ppermute | solution.py:43
  78.2 42.8 %collective-permute-start.14 = (bf16[2048,256]{1,0:T(8,128)(2,1)S(1)}, bf16[2048,256]{1,0:T(8,128)(2,1)S(1)}, u32[]{:S(2)}, u32[]{:S(2)}) collective-permute-start(bf16[2048,256]{1,0:T(8,128)(2,1)S(1)} %collective-permute-done.12.refs_1_), channel_id=1, source_target_pairs={{0,4},{4,0},{1,5},{5,1},{2,6},{6,2},{3,7},{7,3},{8,12},{12,8},{9,1... | collective-permute-start | bytes 3145736 | tf_op jit(solution)/shard_map/ppermute | solution.py:30
  82.5 7.8 %collective-permute-start.22 = (bf16[160,256]{1,0:T(8,128)(2,1)S(1)}, bf16[160,256]{1,0:T(8,128)(2,1)S(1)}, u32[]{:S(2)}, u32[]{:S(2)}) collective-permute-start(bf16[160,256]{1,0:T(8,128)(2,1)S(1)} %get-tuple-element.27), channel_id=1, source_target_pairs={{0,4},{4,8},{8,12},{12,16},{16,20},{20,24},{24,28},{28,32},{32,36}... | collective-permute-start | bytes 245768 | tf_op jit(solution)/shard_map/ppermute | solution.py:477
  91.7 6.3 %collective-permute-start.29 = (bf16[256,256]{1,0:T(8,128)(2,1)S(1)}, bf16[256,256]{1,0:T(8,128)(2,1)S(1)}, u32[]{:S(2)}, u32[]{:S(2)}) collective-permute-start(bf16[256,256]{1,0:T(8,128)(2,1)S(1)} %get-tuple-element.34), channel_id=1, source_target_pairs={{0,1},{1,2},{2,3},{3,0},{4,5},{5,6},{6,7},{7,4},{8,9},{9,10},{10,1... | collective-permute-start | bytes 393224 | tf_op jit(solution)/shard_map/ppermute | solution.py:90
  91.8 29.3 %collective-permute-start.15 = (bf16[1024,256]{1,0:T(8,128)(2,1)S(1)}, bf16[1024,256]{1,0:T(8,128)(2,1)S(1)}, u32[]{:S(2)}, u32[]{:S(2)}) collective-permute-start(bf16[1024,256]{1,0:T(8,128)(2,1)S(1)} %collective-permute-done.13.refs_2_), channel_id=1, source_target_pairs={{0,4},{4,0},{1,5},{5,1},{2,6},{6,2},{3,7},{7,3},{8,12},{12,8},{9,1... | collective-permute-start | bytes 1572872 | tf_op jit(solution)/shard_map/ppermute | solution.py:30
  97.9 6.5 %collective-permute-start.30 = (bf16[256,256]{1,0:T(8,128)(2,1)S(1)}, bf16[256,256]{1,0:T(8,128)(2,1)S(1)}, u32[]{:S(2)}, u32[]{:S(2)}) collective-permute-start(bf16[256,256]{1,0:T(8,128)(2,1)S(1)} %get-tuple-element.35), channel_id=1, source_target_pairs={{0,2},{1,3},{2,0},{3,1},{4,6},{5,7},{6,4},{7,5},{8,10},{9,11},{10,... | collective-permute-start | bytes 393224 | tf_op jit(solution)/shard_map/ppermute | solution.py:90
  104.4 6.3 %collective-permute-start.31 = (bf16[256,256]{1,0:T(8,128)(2,1)S(1)}, bf16[256,256]{1,0:T(8,128)(2,1)S(1)}, u32[]{:S(2)}, u32[]{:S(2)}) collective-permute-start(bf16[256,256]{1,0:T(8,128)(2,1)S(1)} %get-tuple-element.36), channel_id=1, source_target_pairs={{0,3},{1,0},{2,1},{3,2},{4,7},{5,4},{6,5},{7,6},{8,11},{9,8},{10,9... | collective-permute-start | bytes 393224 | tf_op jit(solution)/shard_map/ppermute | solution.py:90
  110.7 8.1 %collective-permute-start.23 = (bf16[272,256]{1,0:T(8,128)(2,1)S(1)}, bf16[272,256]{1,0:T(8,128)(2,1)S(1)}, u32[]{:S(2)}, u32[]{:S(2)}) collective-permute-start(bf16[272,256]{1,0:T(8,128)(2,1)S(1)} %get-tuple-element.29), channel_id=1, source_target_pairs={{0,1},{1,2},{2,3},{3,0},{4,5},{5,6},{6,7},{7,4},{8,9},{9,10},{10,1... | collective-permute-start | bytes 417800 | tf_op jit(solution)/shard_map/ppermute | solution.py:90
  110.8 10.0 %collective-permute-start.24 = (bf16[272,256]{1,0:T(8,128)(2,1)S(1)}, bf16[272,256]{1,0:T(8,128)(2,1)S(1)}, u32[]{:S(2)}, u32[]{:S(2)}) collective-permute-start(bf16[272,256]{1,0:T(8,128)(2,1)S(1)} %get-tuple-element.30), channel_id=1, source_target_pairs={{0,2},{1,3},{2,0},{3,1},{4,6},{5,7},{6,4},{7,5},{8,10},{9,11},{10,... | collective-permute-start | bytes 417800 | tf_op jit(solution)/shard_map/ppermute | solution.py:90
  115.0 6.0 %collective-permute-start.25 = (bf16[272,256]{1,0:T(8,128)(2,1)S(1)}, bf16[272,256]{1,0:T(8,128)(2,1)S(1)}, u32[]{:S(2)}, u32[]{:S(2)}) collective-permute-start(bf16[272,256]{1,0:T(8,128)(2,1)S(1)} %get-tuple-element.31), channel_id=1, source_target_pairs={{0,3},{1,0},{2,1},{3,2},{4,7},{5,4},{6,5},{7,6},{8,11},{9,8},{10,9... | collective-permute-start | bytes 417800 | tf_op jit(solution)/shard_map/ppermute | solution.py:90
  (9 other events, 86.9 us)
